TPU v7x, 32 devices: a whole 2x2x4 slice. The times are simulated.
32 devices in a mesh: sp: 16 (over z, y, x), tp: 2 (over core).
Axes of the slice: x: 2, y: 2, z: 4, core: 2. Of those that a mesh axis runs over, the one named last changes fastest.
Arguments:
- tokens: bfloat16 [4096, 2048], P(('sp', 'tp')), may hold values from -6 to 6
- mix_gain: float32 [2048], replicated, may hold values from 0.1 to 1.9
- query_proj: bfloat16 [2048, 1536], P(None, 'tp'), may hold values from -4 to 4
- compressed_projection: bfloat16 [2048, 256], replicated, may hold values from -0.125 to 0.125
- compressed_norm_gain: float32 [256], replicated, may hold values from 0.1 to 1.9
- rope_proj: bfloat16 [2048, 64], replicated, may hold values from -0.125 to 0.125
- key_up: bfloat16 [256, 1024], P(None, 'tp'), may hold values from -4 to 4
- value_up_weight: bfloat16 [256, 1024], P(None, 'tp'), may hold values from -0.375 to 0.375
- scan_input: bfloat16 [2048, 2048], P('sp', 'tp'), may hold values from -0.125 to 0.125
- scan_gate: bfloat16 [2048, 2048], P('sp', 'tp'), may hold values from -0.125 to 0.125
- scan_write: bfloat16 [2048, 1024], P('sp', 'tp'), may hold values from -0.125 to 0.125
- scan_read: bfloat16 [2048, 1024], P('sp', 'tp'), may hold values from -0.125 to 0.125
- step_proj: bfloat16 [2048, 32], replicated, may hold values from -0.125 to 0.125
- conv_input: bfloat16 [4, 2048], P(None, 'tp'), may hold values from -3 to 3
- conv_write: bfloat16 [4, 1024], P(None, 'tp'), may hold values from -3 to 3
- conv_read: bfloat16 [4, 1024], P(None, 'tp'), may hold values from -3 to 3
- decay_log: float32 [32], P('tp'), may hold values from -16 to -2.8
- decay_offset: float32 [4096, 32], P('sp', 'tp'), may hold values from -2.2 to 0
- skip_gain: float32 [32], P('tp'), may hold values from 0.1 to 1.9
- group_gain: float32 [2048], P('tp'), may hold values from 0.1 to 1.9
Outputs:
- attended: bfloat16 [4096, 1024], P('sp', 'tp')
- scanned: bfloat16 [4096, 2048], P('sp', 'tp')
All inputs are finite; a program needn't handle non-finite values.
Results may differ from a plain program's by a relative error of at most 0.017.
The roundings to bfloat16 on the way count: a program that leaves them out, or rounds other values in their place, can miss the bound.
Values may be sent and summed in bfloat16 or wider, within the bound.
A program may use at most 128 MiB of HBM per device.

v0:
```python
import jax
import jax.numpy as jnp
from jax import lax
from jax.sharding import PartitionSpec as P

UNROTATED_WIDTH = 128
ROPE = 64
VALUE_WIDTH = 128
SSM_DIM = 64
SSM_STATE = 128
BLOCK = 128


eps = 1e-06
theta = 10000.0
floor_score = -1e30


def from_behind(value, axis, steps):
    count = lax.axis_size(axis)
    initial, last = (max(0, -steps), min(count, count - steps))
    return lax.ppermute(value, axis, [(source, source + steps) for source in range(initial, last)])


def entering(array, axis, combine, identity):
    devices, here = (lax.axis_size(axis), lax.axis_index(axis))
    everything = jax.tree.map(
        lambda part, kind: lax.all_gather(part.astype(kind), axis),
        array,
        (jnp.bfloat16, jnp.bfloat16),
    )
    start = jax.tree.map(
        lambda part, zero: jnp.broadcast_to(jnp.asarray(zero, part.dtype), part.shape),
        array,
        identity,
    )

    def turn(k, before):
        reached = k < here
        new = combine(
            before, jax.tree.map(lambda part, own: part[k].astype(own.dtype), everything, array)
        )
        return jax.tree.map(lambda a, b: jnp.where(reached, a, b), new, before)

    return lax.fori_loop(0, devices, turn, start)


def rms_scale(values, gain):
    wide = values.astype(jnp.float32)
    return wide * lax.rsqrt(jnp.mean(wide * wide, axis=-1, keepdims=True) + eps) * gain


def rotate(values, positions):
    half = values.shape[-1] // 2
    freqs = theta ** (-jnp.arange(half, dtype=jnp.float32) * 2.0 / values.shape[-1])
    angle = positions.astype(jnp.float32)[:, None] * freqs[None, :]
    cosine = jnp.cos(angle)
    sine = jnp.sin(angle)
    if values.ndim == 3:
        cosine = cosine[:, None, :]
        sine = sine[:, None, :]
    first = values[..., :half]
    second = values[..., half:]
    return jnp.concatenate(
        [first * cosine - second * sine, second * cosine + first * sine], axis=-1
    )


def short_conv(values, edge, taps):
    span = taps.shape[0]
    length = values.shape[0]
    padded = jnp.concatenate([edge, values], axis=0).astype(jnp.float32)
    result = jnp.zeros(values.shape, jnp.float32)
    for index in range(span):
        result = result + taps[index].astype(jnp.float32)[None, :] * padded[index : index + length]
    return jax.nn.silu(result).astype(jnp.bfloat16)


def blockwise_scan(heads, steps, decays, writes, reads, state, block):
    count = heads.shape[0] // block
    best = lax.Precision.HIGHEST

    def split(values):
        return values.reshape((count, block) + values.shape[1:])

    def one_block(state, inputs):
        head_block, step_block, decay_block, write_block, read_block = inputs
        running = jnp.cumsum(decay_block, axis=0)
        causal = jnp.tril(jnp.ones((block, block), dtype=bool))[:, :, None, None]
        spread = running[:, None] - running[None, :]
        fading = jnp.where(causal, jnp.exp(jnp.where(causal, spread, 0.0)), 0.0)
        inner = jnp.einsum("lgn,sgn->lsg", read_block, write_block, precision=best)
        mixing = inner[..., None] * fading * step_block[None]
        within = jnp.einsum("lsgr,sgrp->lgrp", mixing, head_block, precision=best)
        carried = (
            jnp.einsum("lgn,grpn->lgrp", read_block, state, precision=best)
            * jnp.exp(running)[..., None]
        )
        to_end = jnp.exp(running[-1:] - running) * step_block
        update = jnp.einsum("sgn,sgr,sgrp->grpn", write_block, to_end, head_block, precision=best)
        state = jnp.exp(running[-1])[..., None, None] * state + update
        return (state, within + carried)

    state, outputs = lax.scan(
        one_block, state, (split(heads), split(steps), split(decays), split(writes), split(reads))
    )
    return (state, outputs.reshape(heads.shape))


def gated_norm(mixed, gate, gain):
    length = mixed.shape[0]
    groups = mixed.shape[1]
    flat = mixed.reshape(length, groups, -1)
    gated = flat * jax.nn.silu(gate.astype(jnp.float32)).reshape(length, groups, -1)
    scaled = gated * lax.rsqrt(jnp.mean(gated * gated, axis=-1, keepdims=True) + eps)
    return (scaled * gain.reshape(groups, -1)[None]).reshape(length, -1).astype(jnp.bfloat16)


def attend_piece(
    carry,
    query_plain,
    query_turned,
    query_positions,
    latent,
    key_turned,
    key_positions,
    key_up,
    value_up_weight,
):
    highest, total, summed = carry
    heads = query_plain.shape[1]
    count = latent.shape[0]
    key_plain = (
        jnp.dot(latent, key_up, preferred_element_type=jnp.float32)
        .astype(jnp.bfloat16)
        .reshape(count, heads, -1)
    )
    values = (
        jnp.dot(latent, value_up_weight, preferred_element_type=jnp.float32)
        .astype(jnp.bfloat16)
        .reshape(count, heads, -1)
    )
    scale = (query_plain.shape[-1] + query_turned.shape[-1]) ** (-0.5)
    query_whole = jnp.concatenate([query_plain, query_turned], axis=-1)
    shared_turned = jnp.broadcast_to(key_turned[:, None, :], (count, heads, key_turned.shape[-1]))
    key_whole = jnp.concatenate([key_plain, shared_turned], axis=-1)
    scores = (
        jnp.einsum("qhd,khd->hqk", query_whole, key_whole, preferred_element_type=jnp.float32)
        * scale
    )
    scores = jnp.where(
        key_positions[None, None, :] <= query_positions[None, :, None], scores, -jnp.inf
    )
    new_highest = jnp.maximum(highest, jnp.max(scores, axis=-1))
    weights = jnp.exp(scores - new_highest[..., None])
    total = jnp.sum(weights, axis=-1)
    summed = jnp.einsum(
        "hqk,khd->hqd", weights.astype(jnp.bfloat16), values, preferred_element_type=jnp.float32
    )
    return (new_highest, total, summed)


def shards(
    tokens,
    mix_gain,
    query_proj,
    compressed_projection,
    compressed_norm_gain,
    rope_proj,
    key_up,
    value_up_weight,
    scan_input,
    scan_gate,
    scan_write,
    scan_read,
    step_proj,
    conv_input,
    conv_write,
    conv_read,
    decay_log,
    decay_offset,
    skip_gain,
    group_gain,
):
    own_normed = rms_scale(tokens, mix_gain).astype(jnp.bfloat16)
    rows = lax.all_gather(own_normed, "tp", axis=0, tiled=True)
    length = rows.shape[0]
    sp_index = lax.axis_index("sp")
    positions = sp_index * length + jnp.arange(length, dtype=jnp.int32)
    heads = key_up.shape[1] // UNROTATED_WIDTH
    query = jnp.dot(rows, query_proj, preferred_element_type=jnp.float32).astype(jnp.bfloat16)
    query = query.reshape(length, heads, UNROTATED_WIDTH + ROPE)
    query_plain = query[:, :, :UNROTATED_WIDTH]
    query_turned = rotate(query[:, :, UNROTATED_WIDTH:].astype(jnp.float32), positions).astype(
        jnp.bfloat16
    )
    last_position = sp_index * length + length - 1
    initial_recurrent = (
        jnp.full((heads, length), floor_score, jnp.float32),
        jnp.zeros((heads, length), jnp.float32),
        jnp.zeros((heads, length, VALUE_WIDTH), jnp.float32),
    )
    latent = rms_scale(
        jnp.dot(rows, compressed_projection, preferred_element_type=jnp.float32),
        compressed_norm_gain,
    ).astype(jnp.bfloat16)
    key_turned = rotate(
        jnp.dot(rows, rope_proj, preferred_element_type=jnp.float32), positions
    ).astype(jnp.bfloat16)
    piece = (
        lax.all_gather(latent, "sp", axis=0, tiled=True),
        lax.all_gather(key_turned, "sp", axis=0, tiled=True),
    )
    visit_latent, visit_key_turned = piece
    key_positions = jnp.arange(visit_latent.shape[0], dtype=jnp.int32)

    def work(state):
        return attend_piece(
            state,
            query_plain,
            query_turned,
            positions,
            visit_latent,
            visit_key_turned,
            key_positions,
            key_up,
            value_up_weight,
        )

    def keep(state):
        return state

    highest, total, summed = lax.cond(jnp.int32(0) > last_position, keep, work, initial_recurrent)
    attended = jnp.transpose((summed / total[..., None]).astype(jnp.bfloat16), (1, 0, 2)).reshape(
        length, heads * VALUE_WIDTH
    )
    pieces = (
        lax.all_gather(scan_input, "sp", axis=0, tiled=True),
        lax.all_gather(scan_gate, "sp", axis=0, tiled=True),
        lax.all_gather(scan_write, "sp", axis=0, tiled=True),
        lax.all_gather(scan_read, "sp", axis=0, tiled=True),
    )
    head_sum, gate_sum, write_sum, read_sum = tuple(
        (jnp.dot(rows, piece, preferred_element_type=jnp.float32) for piece in pieces)
    )
    head_raw = head_sum.astype(jnp.bfloat16)
    gate = gate_sum.astype(jnp.bfloat16)
    write_raw = write_sum.astype(jnp.bfloat16)
    read_raw = read_sum.astype(jnp.bfloat16)
    local_heads = decay_log.shape[0]
    step_all = jnp.dot(rows, step_proj, preferred_element_type=jnp.float32)
    step_size = jax.nn.softplus(
        lax.dynamic_slice_in_dim(step_all, lax.axis_index("tp") * local_heads, local_heads, 1)
    )
    span = conv_input.shape[0] - 1
    edge_head, edge_write, boundary_fetch = from_behind(
        (head_raw[length - span :], write_raw[length - span :], read_raw[length - span :]), "sp", 1
    )
    head_conv = short_conv(head_raw, edge_head, conv_input)
    writes = short_conv(write_raw, edge_write, conv_write)
    reads = short_conv(read_raw, boundary_fetch, conv_read)
    groups = scan_write.shape[1] // SSM_STATE
    per_group = local_heads // groups
    log_decay = -jnp.exp(decay_log)[None, :] * step_size + decay_offset
    head_values = head_conv.astype(jnp.float32).reshape(length, groups, per_group, SSM_DIM)
    step_values = step_size.reshape(length, groups, per_group)
    decay_values = log_decay.reshape(length, groups, per_group)
    write_values = writes.astype(jnp.float32).reshape(length, groups, SSM_STATE)
    output_entries = reads.astype(jnp.float32).reshape(length, groups, SSM_STATE)
    empty_state = jnp.zeros((groups, per_group, SSM_DIM, SSM_STATE), jnp.float32)
    final_state, mixed = blockwise_scan(
        head_values, step_values, decay_values, write_values, output_entries, empty_state, BLOCK
    )
    total_decay = jnp.exp(jnp.sum(decay_values, axis=0))

    def chain(earlier, later):
        return (earlier[0] * later[0], later[0][..., None, None] * earlier[1] + later[1])

    prefix = entering(
        (total_decay, final_state),
        "sp",
        chain,
        (jnp.ones_like(total_decay), jnp.zeros_like(final_state)),
    )
    incoming = prefix[1]
    reach = jnp.exp(jnp.cumsum(decay_values, axis=0))
    mixed = (
        mixed
        + jnp.einsum("lgn,grpn->lgrp", output_entries, incoming, precision=lax.Precision.HIGHEST)
        * reach[..., None]
    )
    mixed = mixed + skip_gain.reshape(groups, per_group)[None, :, :, None] * head_values
    scanned = gated_norm(mixed, gate, group_gain)
    return (attended, scanned)


def solution(mesh):
    in_specs = (
        P(("sp", "tp"), None),
        P(),
        P(None, "tp"),
        P(),
        P(),
        P(),
        P(None, "tp"),
        P(None, "tp"),
        P("sp", "tp"),
        P("sp", "tp"),
        P("sp", "tp"),
        P("sp", "tp"),
        P(),
        P(None, "tp"),
        P(None, "tp"),
        P(None, "tp"),
        P("tp"),
        P("sp", "tp"),
        P("tp"),
        P("tp"),
    )
    out_specs = (P("sp", "tp"), P("sp", "tp"))
    return jax.shard_map(shards, mesh=mesh, in_specs=in_specs, out_specs=out_specs, check_vma=False)
```

profile of v0, /device:TPU:0, one launch (start us, length us, event | category | flops | bytes accessed | tf_op | source)
XLA Modules:
  0.0 502.8 jit_solution(1909801481627099106)
XLA Ops:
  12.9 9.8 %all-gather.9.cloned.1.call-done = bf16[256,2048]{1,0:T(8,128)(2,1)} async-done(((bf16[128,2048]{1,0:T(8,128)(2,1)}), bf16[256,2048]{1,0:T(8,128)(2,1)}) %all-gather.9.cloned.1.call-update) | async-done | bytes 1048592 | tf_op jit(solution)/shard_map/all_gather | solution.py:186
  28.2 58.9 %all-gather.17.cloned.1.call-done = bf16[2048,512]{1,0:T(8,128)(2,1)} async-done(((bf16[128,512]{1,0:T(8,128)(2,1)}), bf16[2048,512]{1,0:T(8,128)(2,1)}) %all-gather.17.cloned.1.call-update) | async-done | bytes 2097168 | tf_op jit(solution)/shard_map/all_gather | solution.py:241
  89.7 3.2 collective-permute-start.2
  92.9 56.2 %all-gather.15.cloned.1.call-done = bf16[2048,512]{1,0:T(8,128)(2,1)} async-done(((bf16[128,512]{1,0:T(8,128)(2,1)}), bf16[2048,512]{1,0:T(8,128)(2,1)}) %all-gather.15.cloned.1.call-update) | async-done | bytes 2097168 | tf_op jit(solution)/shard_map/all_gather | solution.py:240
  157.4 68.7 %all-gather.13.cloned.1.call-done = bf16[2048,1024]{1,0:T(8,128)(2,1)} async-done(((bf16[128,1024]{1,0:T(8,128)(2,1)}), bf16[2048,1024]{1,0:T(8,128)(2,1)}) %all-gather.13.cloned.1.call-update) | async-done | bytes 4194320 | tf_op jit(solution)/shard_map/all_gather | solution.py:238
  226.1 3.8 convolution_convert_fusion.3
  229.9 3.5 collective-permute-start
  239.7 3.5 reshape.255
  246.1 71.1 %while.27 = (s32[]{:T(128)}, f32[4,4,64,128]{3,2,1,0:T(8,128)}, f32[2,128,4,4,64]{1,0,4,3,2:T(2,128)}, f32[2,128,4,4]{1,0,3,2:T(2,128)S(1)}, f32[2,128,4,4]{1,0,...) while((s32[]{:T(128)}, f32[4,4,64,128]{3,2,1,0:T(8,128)}, ...), condition=%wide.region_8.9_spmd.clone, body=%wide.region_6.8_spmd.clone.sunk | while | flops 707151872 | bytes 8627708 | solution.py:104
  260.4 4.3 fusion.130
  264.7 13.1 %dynamic_update_slice.6 = f32[2,128,4,4,64]{1,0,4,3,2:T(2,128)} dynamic-update-slice(f32[2,128,4,4,64]{1,0,4,3,2:T(2,128)} %get-tuple-element.443, f32[1,128,4,4,64]{1,0,4,3,2:T(1,128)} %bitcast.160, s32[]{:T(128)} %get-tuple-element.441, s32[]{:T(128)} %constant.101.clone.1..sunk, s32[]{:T(128)} %constant.101.clone.1..sunk, s32[]{:T(128)} %constant.101.clone.1..sunk, s32[]{:T(128)} %constant.101.clone.1..sunk) | dynamic-update-slice | bytes 1048580 | tf_op jit(solution)/shard_map/while/body/jit(dynamic_update_index_in_dim)/dynamic_update_slice | solution.py:104
  296.0 4.3 fusion.130
  300.3 13.1 %dynamic_update_slice.6 = f32[2,128,4,4,64]{1,0,4,3,2:T(2,128)} dynamic-update-slice(f32[2,128,4,4,64]{1,0,4,3,2:T(2,128)} %get-tuple-element.443, f32[1,128,4,4,64]{1,0,4,3,2:T(1,128)} %bitcast.160, s32[]{:T(128)} %get-tuple-element.441, s32[]{:T(128)} %constant.101.clone.1..sunk, s32[]{:T(128)} %constant.101.clone.1..sunk, s32[]{:T(128)} %constant.101.clone.1..sunk, s32[]{:T(128)} %constant.101.clone.1..sunk) | dynamic-update-slice | bytes 1048580 | tf_op jit(solution)/shard_map/while/body/jit(dynamic_update_index_in_dim)/dynamic_update_slice | solution.py:104
  319.8 4.8 reduce-window.6
  329.4 39.7 %all_gather.37 = bf16[16,4,4]{2,1,0:T(4,128)(2,1)} all-gather(bf16[1,4,4]{2,1,0:T(4,128)(2,1)S(1)} %convert_element_type.164), channel_id=1, replica_groups=mesh['sp'=16,'tp'=2] {'sp'}, dimensions={0}, use_global_device_ids=true | all-gather | bytes 544 | tf_op jit(solution)/shard_map/all_gather | solution.py:28
  371.1 40.1 %all_gather.33 = bf16[4096,64]{0,1:T(8,128)(2,1)S(1)} all-gather(bf16[256,64]{0,1:T(8,128)(2,1)S(1)} %pad_maximum_fusion.1), channel_id=1, replica_groups=mesh['sp'=16,'tp'=2] {'sp'}, dimensions={0}, use_global_device_ids=true | all-gather | bytes 557056 | tf_op jit(solution)/shard_map/all_gather | solution.py:212
  412.0 33.8 %conditional.1 = (f32[4,256]{1,0:T(4,128)S(1)}, f32[4,256,128]{2,1,0:T(8,128)S(1)}) conditional(s32[]{:T(128)} %convert_element_type.145, (s32[4096]{0:T(1024)S(1)}, s32[]{:T(128)}, s32[256]{0:T(256)S(1)}, bf16[256,4,192]{0,2,1:T(8,128)(2,1)S(1)}, bf16[256,4,64]{0,2,1:T(8,128)(2,1)S(1)}, /*index=5*/bf16[4096,256]{0,1:T(8,128)(2,1)}, ...), branch_computations={%region_2.5_spmd, %region_5.6_spmd} | conditional | flops 4896586752 | bytes 100052104 | solution.py:233
  412.7 3.3 convolution_convert_fusion.1
  416.3 8.1 %fusion = (f32[4,256]{1,0:T(4,128)S(1)}, f32[4,256,4096]{2,1,0:T(8,128)}) fusion(pred[256,4096]{1,0:T(8,128)(4,1)S(1)} %broadcast_compare_fusion, bf16[4096,4,64]{0,2,1:T(8,128)(2,1)S(1)} %broadcast_in_dim.42, bf16[4096,4,128]{0,2,1:T(8,128)(2,1)S(1)} %bitcast.161, bf16[256,4,64]{0,2,1:T(8,128)(2,1)S(1)} %get-tuple-element.144, ...), kind=kOutput, calls=%fused_computation.2 | convolution fusion | flops 1636563968 | bytes 24514560 | tf_op jit(solution)/shard_map/cond/branch_0_fun/qhd,khd->hqk/dot_general | solution.py:148
  424.4 3.3 convolution_convert_fusion
  427.7 10.0 %fusion.3 = f32[4,256,128]{2,1,0:T(8,128)S(1)} fusion(bf16[4096,4,128]{0,2,1:T(8,128)(2,1)} %bitcast.162, f32[4,256,4096]{2,1,0:T(8,128)} %get-tuple-element.306, f32[4,256]{1,0:T(4,128)S(1)} %broadcast_maximum_fusion, pred[256,4096]{1,0:T(8,128)(4,1)} %copy-done.7), kind=kOutput, calls=%fused_computation.5 | convolution fusion | flops 1090519040 | bytes 22548480 | tf_op jit(solution)/shard_map/cond/branch_0_fun/hqk,khd->hqd/dot_general | solution.py:157
  437.7 8.1 %fusion.2 = f32[4,256]{1,0:T(4,128)S(1)} fusion(f32[4,256,4096]{2,1,0:T(8,128)} %get-tuple-element.306, f32[4,256]{1,0:T(4,128)S(1)} %broadcast_maximum_fusion, pred[256,4096]{1,0:T(8,128)(4,1)S(1)} %copy-done.8), kind=kLoop, calls=%fused_computation.4 | loop fusion | flops 16776192 | bytes 17833984 | tf_op jit(solution)/shard_map/cond/branch_0_fun/reduce_sum | solution.py:156
  446.8 4.6 convert_multiply_fusion
  457.5 28.2 %while.28 = (s32[]{:T(128)}, f32[4,4,64,128]{3,2,1,0:T(8,128)S(1)}, s32[]{:T(128)}, bf16[16,4,4]{2,1,0:T(4,128)(2,1)}, bf16[16,4,4,64,128]{4,3,2,1,0:T(8,128)(2,1)}, /*index=5*/s32[]{:T(128)}, s32[]{:T(128)}) while((s32[]{:T(128)}, f32[4,4,64,128]{3,2,1,0:T(8,128)S(1)}, s32[]{:T(128)}, bf16[16,4,4]{2,1,0:T(4,128)(2,1)}, ...), condition=%wide.region_11.12_spmd.clone, body=%wide.region_10.11_spmd.clone.sunk | while | flops 655380 | bytes 1310985 | solution.py:45
  (212 shorter events, 123.3 us)
Async XLA Ops:
  7.2 317.9 %copy-start = (bf16[2048,768]{1,0:T(8,128)(2,1)S(1)}, bf16[2048,768]{1,0:T(8,128)(2,1)}, u32[]{:S(2)}) copy-start(bf16[2048,768]{1,0:T(8,128)(2,1)} %param.28) | copy-start | bytes 9437188
  7.2 19.0 %copy-start.18 = (bf16[4,512]{1,0:T(4,128)(2,1)S(1)}, bf16[4,512]{1,0:T(4,128)(2,1)}, u32[]{:S(2)}) copy-start(bf16[4,512]{1,0:T(4,128)(2,1)} %param.41) | copy-start | bytes 12292
  7.2 19.0 %copy-start.25 = (f32[16]{0:T(128)S(1)}, f32[16]{0:T(128)}, u32[]{:S(2)}) copy-start(f32[16]{0:T(128)} %param.42) | copy-start | bytes 196
  7.2 19.0 %copy-start.19 = (bf16[4,512]{1,0:T(4,128)(2,1)S(1)}, bf16[4,512]{1,0:T(4,128)(2,1)}, u32[]{:S(2)}) copy-start(bf16[4,512]{1,0:T(4,128)(2,1)} %param.40) | copy-start | bytes 12292
  7.2 19.0 %copy-start.17 = (bf16[4,1024]{1,0:T(4,128)(2,1)S(1)}, bf16[4,1024]{1,0:T(4,128)(2,1)}, u32[]{:S(2)}) copy-start(bf16[4,1024]{1,0:T(4,128)(2,1)} %param.39) | copy-start | bytes 24580
  7.2 19.1 %copy-start.16 = (bf16[2048,32]{0,1:T(8,128)(2,1)S(1)}, bf16[2048,32]{0,1:T(8,128)(2,1)}, u32[]{:S(2)}) copy-start(bf16[2048,32]{0,1:T(8,128)(2,1)} %param.38) | copy-start | bytes 393220
  7.2 20.7 %copy-start.20 = (f32[256,16]{0,1:T(8,128)S(1)}, f32[256,16]{0,1:T(8,128)}, u32[]{:S(2)}) copy-start(f32[256,16]{0,1:T(8,128)} %param.43) | copy-start | bytes 49156
  7.3 15.4 %all-gather.9.cloned.1.call-start = ((), (), s32[]{:S(2)}) async-start(), calls=%async_computation | async-start | bytes 1572864 | tf_op jit(solution)/shard_map/all_gather | solution.py:186
  10.7 76.3 %all-gather.17.cloned.1.call-start = ((), (), s32[]{:S(2)}) async-start(), calls=%async_computation.4 | async-start | bytes 2228224 | tf_op jit(solution)/shard_map/all_gather | solution.py:241
  11.5 137.6 %all-gather.15.cloned.1.call-start = ((), (), s32[]{:S(2)}) async-start(), calls=%async_computation.3 | async-start | bytes 2228224 | tf_op jit(solution)/shard_map/all_gather | solution.py:240
  12.2 213.9 %all-gather.13.cloned.1.call-start = ((), (), s32[]{:S(2)}) async-start(), calls=%async_computation.2 | async-start | bytes 4456448 | tf_op jit(solution)/shard_map/all_gather | solution.py:238
  12.8 399.2 %all-gather.11.cloned.1.call-start = ((), (), s32[]{:S(2)}) async-start(), calls=%async_computation.1 | async-start | bytes 2228224 | tf_op jit(solution)/shard_map/all_gather | solution.py:211
  25.5 421.2 %all-gather.19.cloned.1.call-start = ((), (), s32[]{:S(2)}) async-start(), calls=%async_computation.5 | async-start | bytes 4456448 | tf_op jit(solution)/shard_map/all_gather | solution.py:239
  26.1 431.4 %all-gather.21.cloned.1.call-start = ((), (), s32[]{:S(2)}) async-start(), calls=%async_computation.6 | async-start | bytes 4456448 | tf_op jit(solution)/shard_map/all_gather | solution.py:28
  89.7 65.2 %collective-permute-start.2 = (bf16[3,512]{1,0:T(4,128)(2,1)S(1)}, bf16[3,512]{1,0:T(4,128)(2,1)S(1)}, u32[]{:S(2)}, u32[]{:S(2)}) collective-permute-start(bf16[3,512]{1,0:T(4,128)(2,1)S(1)} %slice.161), channel_id=1, source_target_pairs={{0,2},{2,4},{4,6},{6,8},{8,10},{10,12},{12,14},{14,16},{16,18},{18... | collective-permute-start | bytes 9224 | tf_op jit(solution)/shard_map/ppermute | solution.py:22
  151.7 4.5 collective-permute-start.1
  229.9 7.0 %collective-permute-start = (bf16[3,1024]{1,0:T(4,128)(2,1)S(1)}, bf16[3,1024]{1,0:T(4,128)(2,1)S(1)}, u32[]{:S(2)}, u32[]{:S(2)}) collective-permute-start(bf16[3,1024]{1,0:T(4,128)(2,1)S(1)} %slice.151), channel_id=1, source_target_pairs={{0,2},{2,4},{4,6},{6,8},{8,10},{10,12},{12,14},{14,16},{16,18},{18... | collective-permute-start | bytes 18440 | tf_op jit(solution)/shard_map/ppermute | solution.py:22
  246.1 72.9 %copy-start.24 = (f32[16]{0:T(128)S(1)}, f32[16]{0:T(128)}, u32[]{:S(2)}) copy-start(f32[16]{0:T(128)} %param.44) | copy-start | bytes 196
  325.1 86.1 %copy-start.11 = (bf16[256,512]{1,0:T(8,128)(2,1)S(1)}, bf16[256,512]{1,0:T(8,128)(2,1)}, u32[]{:S(2)}) copy-start(bf16[256,512]{1,0:T(8,128)(2,1)} %copy-done.10) | copy-start | bytes 786436
  328.2 83.8 %copy-start.14 = (bf16[256,512]{1,0:T(8,128)(2,1)S(1)}, bf16[256,512]{1,0:T(8,128)(2,1)}, u32[]{:S(2)}) copy-start(bf16[256,512]{1,0:T(8,128)(2,1)} %param.32) | copy-start | bytes 786436
  412.0 34.8 %copy-start.6 = (bf16[256,2048]{1,0:T(8,128)(2,1)S(1)}, bf16[256,2048]{1,0:T(8,128)(2,1)}, u32[]{:S(2)}) copy-start(bf16[256,2048]{1,0:T(8,128)(2,1)} %all-gather.9.cloned.1.call-done) | copy-start | bytes 3145732
  454.3 31.4 %copy-start.9 = (f32[256,1024]{0,1:T(8,128)S(1)}, f32[256,1024]{0,1:T(8,128)}, u32[]{:S(2)}) copy-start(f32[256,1024]{0,1:T(8,128)} %copy.94) | copy-start | bytes 3145732
  454.3 31.4 %copy-start.12 = (bf16[256,4,128]{2,1,0:T(4,128)(2,1)S(1)}, bf16[256,4,128]{2,1,0:T(4,128)(2,1)}, u32[]{:S(2)}) copy-start(bf16[256,4,128]{2,1,0:T(4,128)(2,1)} %reshape.226) | copy-start | bytes 786436
  454.3 31.4 %copy-start.21 = (f32[4,4]{1,0:T(4,128)S(1)}, f32[4,4]{1,0:T(4,128)}, u32[]{:S(2)}) copy-start(f32[4,4]{1,0:T(4,128)} %mul.482) | copy-start | bytes 196
  (12 other events, 90.9 us)
Sparse Core Ops, SparseCore 0:
  10.9 11.7 all-gather.8
  25.4 61.5 all-gather.16
  89.8 59.1 all-gather.14
  151.7 74.3 all-gather.12
  228.7 63.3 all-gather.10
  294.6 74.9 all-gather.18
  372.4 75.3 all-gather.20
where the time goes:
time: 506 us; the launch traced here: 503 us
  waiting for transfers between devices  196 us (39%)
  blocking collectives  79.8 us (16%)
  matrix products  73.4 us (15%)
  local copies, waits for them, and re-layouts  64.6 us (13%)
  other arithmetic  63.3 us (13%)
  between operations  14.7 us (3%)
  starting transfers between devices  10.2 us (2%)
    all_gather x1, waiting for transfers between devices, shards(): lax.all_gather(scan_input, 'sp', axis=0, tiled=True)  68.7 us
    all_gather x1, waiting for transfers between devices, shards(): lax.all_gather(scan_read, 'sp', axis=0, tiled=True)  58.9 us
    all_gather x1, waiting for transfers between devices, shards(): lax.all_gather(scan_write, 'sp', axis=0, tiled=True)  56.2 us
    all_gather x1, blocking collectives, shards(): lax.all_gather(key_turned, 'sp', axis=0, tiled=True)  40.1 us
    all_gather x1, blocking collectives, entering(): lax.all_gather(part.astype(kind), axis)  39.7 us
    dynamic_update_slice x2, local copies, waits for them, and re-layouts, blockwise_scan(): lax.scan(one_block, state, (split(heads), split(steps), split(decays), sp...  26.2 us
    select_n x16, other arithmetic, turn(): return jax.tree.map(lambda a, b: jnp.where(reached, a, b), new, before)  17.4 us
    dot_general x4, matrix products, shards(): jnp.dot(rows, piece, preferred_element_type=jnp.float32)  13.7 us
  transfers between devices with their start and end apart: 10, of which 5 were waited for; matrix products, arithmetic and copies ran while one was open for 32% of the time, Pallas kernels for 0%

commit v1 on v0

v1 whole, which is shorter than its diff:
```python
import jax
import jax.numpy as jnp
from jax import lax
from jax.sharding import PartitionSpec as P

UNROTATED_WIDTH = 128
ROPE = 64
VALUE_WIDTH = 128
SSM_DIM = 64
SSM_STATE = 128


eps = 1e-06
theta = 10000.0
floor_score = -1e30


def from_behind(value, axis, steps):
    count = lax.axis_size(axis)
    initial, last = (max(0, -steps), min(count, count - steps))
    return lax.ppermute(value, axis, [(source, source + steps) for source in range(initial, last)])


def rms_scale(values, gain):
    wide = values.astype(jnp.float32)
    return wide * lax.rsqrt(jnp.mean(wide * wide, axis=-1, keepdims=True) + eps) * gain


def rotate(values, positions):
    half = values.shape[-1] // 2
    freqs = theta ** (-jnp.arange(half, dtype=jnp.float32) * 2.0 / values.shape[-1])
    angle = positions.astype(jnp.float32)[:, None] * freqs[None, :]
    cosine = jnp.cos(angle)
    sine = jnp.sin(angle)
    if values.ndim == 3:
        cosine = cosine[:, None, :]
        sine = sine[:, None, :]
    first = values[..., :half]
    second = values[..., half:]
    return jnp.concatenate(
        [first * cosine - second * sine, second * cosine + first * sine], axis=-1
    )


def short_conv(values, edge, taps):
    span = taps.shape[0]
    length = values.shape[0]
    padded = jnp.concatenate([edge, values], axis=0).astype(jnp.float32)
    result = jnp.zeros(values.shape, jnp.float32)
    for index in range(span):
        result = result + taps[index].astype(jnp.float32)[None, :] * padded[index : index + length]
    return jax.nn.silu(result).astype(jnp.bfloat16)


def local_scan(heads, steps, decays, writes, reads):
    length = decays.shape[-1]
    running = jnp.einsum(
        "grs,ls->grl",
        decays,
        jnp.tril(jnp.ones((length, length), jnp.float32)),
        precision=lax.Precision.HIGHEST,
    )
    causal = jnp.tril(jnp.ones((length, length), dtype=bool))
    spread = jnp.where(causal, running[..., :, None] - running[..., None, :], -jnp.inf)
    inner = jnp.einsum("gln,gsn->gls", reads, writes, preferred_element_type=jnp.float32)
    mixing = inner[:, None] * jnp.exp(spread) * steps[:, :, None, :]
    within = jnp.einsum(
        "grls,grsp->grlp",
        mixing.astype(jnp.bfloat16),
        heads,
        preferred_element_type=jnp.float32,
    )
    to_end = jnp.exp(running[..., -1:] - running) * steps
    weighted = (heads.astype(jnp.float32) * to_end[..., None]).astype(jnp.bfloat16)
    state = jnp.einsum(
        "grsp,gsn->grpn", weighted, writes, preferred_element_type=jnp.float32
    )
    return running, state, within


def state_before(state, total, axis):
    groups, per_group, dim, entries = state.shape
    count = groups * per_group
    flat = state.reshape(count * dim, entries).astype(jnp.bfloat16)
    high = total.reshape(count).astype(jnp.bfloat16)
    low = (total.reshape(count) - high.astype(jnp.float32)).astype(jnp.bfloat16)
    tail = jnp.zeros((16, entries), jnp.bfloat16)
    tail = tail.at[0, :count].set(high).at[1, :count].set(low)
    everything = lax.all_gather(jnp.concatenate([flat, tail], axis=0), axis)
    here = lax.axis_index(axis)
    devices = everything.shape[0]
    states = everything[:, : count * dim].reshape(devices, count, dim, entries)
    totals = everything[:, count * dim, :count].astype(jnp.float32) + everything[
        :, count * dim + 1, :count
    ].astype(jnp.float32)
    index = jnp.arange(devices)
    between = (index[None, :] > index[:, None]) & (index[None, :] < here)
    path = jnp.sum(jnp.where(between[:, :, None], totals[None], 0.0), axis=1)
    factor = jnp.where((index < here)[:, None], jnp.exp(path), 0.0)
    before = jnp.sum(states.astype(jnp.float32) * factor[:, :, None, None], axis=0)
    return before.reshape(state.shape)


def gated_norm(mixed, gate, gain):
    length = mixed.shape[0]
    groups = mixed.shape[1]
    flat = mixed.reshape(length, groups, -1)
    gated = flat * jax.nn.silu(gate.astype(jnp.float32)).reshape(length, groups, -1)
    scaled = gated * lax.rsqrt(jnp.mean(gated * gated, axis=-1, keepdims=True) + eps)
    return (scaled * gain.reshape(groups, -1)[None]).reshape(length, -1).astype(jnp.bfloat16)


def attend_piece(
    carry,
    query_plain,
    query_turned,
    query_positions,
    latent,
    key_turned,
    key_positions,
    key_up,
    value_up_weight,
):
    highest, total, summed = carry
    heads = query_plain.shape[1]
    count = latent.shape[0]
    key_plain = (
        jnp.dot(latent, key_up, preferred_element_type=jnp.float32)
        .astype(jnp.bfloat16)
        .reshape(count, heads, -1)
    )
    values = (
        jnp.dot(latent, value_up_weight, preferred_element_type=jnp.float32)
        .astype(jnp.bfloat16)
        .reshape(count, heads, -1)
    )
    scale = (query_plain.shape[-1] + query_turned.shape[-1]) ** (-0.5)
    query_whole = jnp.concatenate([query_plain, query_turned], axis=-1)
    shared_turned = jnp.broadcast_to(key_turned[:, None, :], (count, heads, key_turned.shape[-1]))
    key_whole = jnp.concatenate([key_plain, shared_turned], axis=-1)
    scores = (
        jnp.einsum("qhd,khd->hqk", query_whole, key_whole, preferred_element_type=jnp.float32)
        * scale
    )
    scores = jnp.where(
        key_positions[None, None, :] <= query_positions[None, :, None], scores, -jnp.inf
    )
    new_highest = jnp.maximum(highest, jnp.max(scores, axis=-1))
    weights = jnp.exp(scores - new_highest[..., None])
    total = jnp.sum(weights, axis=-1)
    summed = jnp.einsum(
        "hqk,khd->hqd", weights.astype(jnp.bfloat16), values, preferred_element_type=jnp.float32
    )
    return (new_highest, total, summed)


def shards(
    tokens,
    mix_gain,
    query_proj,
    compressed_projection,
    compressed_norm_gain,
    rope_proj,
    key_up,
    value_up_weight,
    scan_input,
    scan_gate,
    scan_write,
    scan_read,
    step_proj,
    conv_input,
    conv_write,
    conv_read,
    decay_log,
    decay_offset,
    skip_gain,
    group_gain,
):
    own_normed = rms_scale(tokens, mix_gain).astype(jnp.bfloat16)
    rows = lax.all_gather(own_normed, "tp", axis=0, tiled=True)
    length = rows.shape[0]
    width = tokens.shape[1]
    sp_index = lax.axis_index("sp")
    positions = sp_index * length + jnp.arange(length, dtype=jnp.int32)
    heads = key_up.shape[1] // UNROTATED_WIDTH
    local_heads = decay_log.shape[0]
    latent_width = compressed_projection.shape[1]
    small = jnp.dot(
        rows,
        jnp.concatenate([compressed_projection, rope_proj, step_proj], axis=1),
        preferred_element_type=jnp.float32,
    )
    latent = rms_scale(small[:, :latent_width], compressed_norm_gain).astype(jnp.bfloat16)
    key_turned = rotate(small[:, latent_width : latent_width + ROPE], positions).astype(
        jnp.bfloat16
    )
    step_all = small[:, latent_width + ROPE :]
    edge_rows = from_behind(rows[length - 8 :], "sp", 1)
    keys = jnp.concatenate([latent, key_turned], axis=1)
    depth = scan_input.shape[0]
    packed = jnp.concatenate(
        [scan_input, scan_gate, scan_write, scan_read, keys.reshape(depth, -1)], axis=1
    )
    everything = lax.all_gather(packed, "sp", axis=0, tiled=True)
    widths = [w.shape[1] for w in (scan_input, scan_gate, scan_write, scan_read)]
    scan_width = sum(widths)
    all_keys = everything[:, scan_width:].reshape(-1, latent_width + ROPE)
    projected = jnp.dot(
        jnp.concatenate([edge_rows, rows], axis=0),
        everything[:, :scan_width],
        preferred_element_type=jnp.float32,
    ).astype(jnp.bfloat16)
    edge, projected = projected[:8], projected[8:]
    gate = projected[:, widths[0] : widths[0] + widths[1]]
    span = conv_input.shape[0] - 1

    def convolved(start, size, taps):
        return short_conv(
            projected[:, start : start + size], edge[8 - span :, start : start + size], taps
        )

    head_conv = convolved(0, widths[0], conv_input)
    writes = convolved(widths[0] + widths[1], widths[2], conv_write)
    reads = convolved(widths[0] + widths[1] + widths[2], widths[3], conv_read)
    step_size = jax.nn.softplus(
        lax.dynamic_slice_in_dim(step_all, lax.axis_index("tp") * local_heads, local_heads, 1)
    )
    groups = scan_write.shape[1] // SSM_STATE
    per_group = local_heads // groups
    log_decay = -jnp.exp(decay_log)[None, :] * step_size + decay_offset
    head_values = jnp.transpose(
        head_conv.reshape(length, groups, per_group, SSM_DIM), (1, 2, 0, 3)
    )
    step_values = step_size.T.reshape(groups, per_group, length)
    decay_values = log_decay.T.reshape(groups, per_group, length)
    write_values = jnp.transpose(writes.reshape(length, groups, SSM_STATE), (1, 0, 2))
    read_values = jnp.transpose(reads.reshape(length, groups, SSM_STATE), (1, 0, 2))
    running, final_state, mixed = local_scan(
        head_values, step_values, decay_values, write_values, read_values
    )
    incoming = state_before(final_state, running[..., -1], "sp")
    carried = jnp.einsum(
        "gln,grpn->grlp",
        read_values,
        incoming.astype(jnp.bfloat16),
        preferred_element_type=jnp.float32,
    )
    mixed = (
        mixed
        + carried * jnp.exp(running)[..., None]
        + skip_gain.reshape(groups, per_group)[:, :, None, None] * head_values.astype(jnp.float32)
    )
    scanned = gated_norm(jnp.transpose(mixed, (2, 0, 1, 3)), gate, group_gain)

    query = jnp.dot(rows, query_proj, preferred_element_type=jnp.float32).astype(jnp.bfloat16)
    query = query.reshape(length, heads, UNROTATED_WIDTH + ROPE)
    query_plain = query[:, :, :UNROTATED_WIDTH]
    query_turned = rotate(query[:, :, UNROTATED_WIDTH:].astype(jnp.float32), positions).astype(
        jnp.bfloat16
    )
    initial = (
        jnp.full((heads, length), floor_score, jnp.float32),
        jnp.zeros((heads, length), jnp.float32),
        jnp.zeros((heads, length, VALUE_WIDTH), jnp.float32),
    )
    key_positions = jnp.arange(all_keys.shape[0], dtype=jnp.int32)
    _, total, summed = attend_piece(
        initial,
        query_plain,
        query_turned,
        positions,
        all_keys[:, :latent_width],
        all_keys[:, latent_width:],
        key_positions,
        key_up,
        value_up_weight,
    )
    attended = jnp.transpose((summed / total[..., None]).astype(jnp.bfloat16), (1, 0, 2)).reshape(
        length, heads * VALUE_WIDTH
    )
    return (attended, scanned)


def solution(mesh):
    in_specs = (
        P(("sp", "tp"), None),
        P(),
        P(None, "tp"),
        P(),
        P(),
        P(),
        P(None, "tp"),
        P(None, "tp"),
        P("sp", "tp"),
        P("sp", "tp"),
        P("sp", "tp"),
        P("sp", "tp"),
        P(),
        P(None, "tp"),
        P(None, "tp"),
        P(None, "tp"),
        P("tp"),
        P("sp", "tp"),
        P("tp"),
        P("tp"),
    )
    out_specs = (P("sp", "tp"), P("sp", "tp"))
    return jax.shard_map(shards, mesh=mesh, in_specs=in_specs, out_specs=out_specs, check_vma=False)
```

time: 506 us -> 322 us (0.64)
  blocking collectives: 79.8 us -> 0 us
  matrix products: 73.4 us -> 37.7 us
  local copies, waits for them, and re-layouts: 64.6 us -> 37.7 us
  other arithmetic: 63.3 us -> 37.4 us
  starting transfers between devices: 10.2 us -> 3.75 us
  waiting for transfers between devices: 196 us -> 190 us
    all_gather x2 -> x0, blocking collectives: 79.8 us -> none  [the longest x1 40.1 us: shards(): lax.all_gather(key_turned, 'sp', axis=0, tiled=True)]
    dot_general x16 -> x7, matrix products: 45.7 us -> 15.2 us  [the longest x1 8.42 us: shards(): jnp.dot(jnp.concatenate([edge_rows, rows], axis=0), everything[:, :scan_w...]
    dynamic_update_slice x2 -> x0, local copies, waits for them, and re-layouts: 26.2 us -> none  [blockwise_scan(): lax.scan(one_block, state, (split(heads), split(steps), split(decays), sp...]
    select_n x16 -> x1, other arithmetic: 17.4 us -> 0.07 us  [state_before(): factor = jnp.where((index < here)[:, None], jnp.exp(path), 0.0)]
    convert_element_type x20 -> x2, other arithmetic: 14.7 us -> 0.78 us  [the longest x1 0.78 us: shards(): rms_scale(small[:, :latent_width], compressed_norm_gain)]
    unnamed x46 -> x80, local copies, waits for them, and re-layouts: 4.07 us -> 14.6 us
    slice x5 -> x6, local copies, waits for them, and re-layouts: 0.24 us -> 8.68 us  [the longest x1 3.49 us: shards(): all_keys = everything[:, scan_width:].reshape(-1, latent_width + ROPE)]
    all_gather x1, waiting for transfers between devices: 9.8 us -> 2.14 us  [shards(): rows = lax.all_gather(own_normed, 'tp', axis=0, tiled=True)]
  transfers between devices with their start and end apart: 10 -> 4, of which waited for: 5 -> 3; matrix products, arithmetic and copies ran while one was open for 32% -> 21% of each run, Pallas kernels for 0% -> 0%
where the time goes in v1:
time: 322 us; the launch traced here: 321 us
  waiting for transfers between devices  190 us (59%)
  local copies, waits for them, and re-layouts  37.7 us (12%)
  matrix products  37.7 us (12%)
  other arithmetic  37.4 us (12%)
  between operations  14.3 us (4%)
  starting transfers between devices  3.75 us (1%)
    all_gather x1, waiting for transfers between devices, shards(): everything = lax.all_gather(packed, 'sp', axis=0, tiled=True)  170 us
    all_gather x1, waiting for transfers between devices, state_before(): everything = lax.all_gather(jnp.concatenate([flat, tail], axis=0), axis)  17.9 us
    unnamed x80, local copies, waits for them, and re-layouts  14.6 us
    dot_general x1, matrix products, shards(): jnp.dot(jnp.concatenate([edge_rows, rows], axis=0), everything[:, :scan_w...  8.42 us
    reduce_sum x1, other arithmetic, attend_piece(): total = jnp.sum(weights, axis=-1)  8.37 us
    dot_general x1, matrix products, attend_piece(): jnp.einsum('qhd,khd->hqk', query_whole, key_whole, preferred_element_type...  7.87 us
    dot_general x1, matrix products, attend_piece(): jnp.einsum('hqk,khd->hqd', weights.astype(jnp.bfloat16), values, preferre...  6.76 us
  transfers between devices with their start and end apart: 4, of which 3 were waited for; matrix products, arithmetic and copies ran while one was open for 21% of the time, Pallas kernels for 0%

profile of v1, /device:TPU:0, one launch (start us, length us, event | category | flops | bytes accessed | tf_op | source)
XLA Modules:
  0.0 320.8 jit_solution(13129641332036617341)
XLA Ops:
  8.6 2.0 fusion.42
  10.7 2.0 copy.58
  20.5 2.1 all-gather.5.cloned.1.call-done
  22.6 3.2 %fusion.24 = f32[256,352]{0,1:T(8,128)S(1)} fusion(bf16[256,2048]{1,0:T(8,128)(2,1)} %all-gather.5.cloned.1.call-done, bf16[2048,32]{1,0:T(8,128)(2,1)} %copy.59, bf16[2048,64]{1,0:T(8,128)(2,1)} %copy.58, bf16[2048,256]{1,0:T(8,128)(2,1)} %param.27), kind=kOutput, calls=%fused_computation.28 | convolution fusion | flops 373424128 | bytes 2850816 | tf_op jit(solution)/shard_map/dot_general | solution.py:188
  30.8 3.6 %collective-permute-start = (bf16[8,2048]{1,0:T(8,128)(2,1)S(1)}, bf16[8,2048]{1,0:T(8,128)(2,1)S(1)}, u32[]{:S(2)}, u32[]{:S(2)}) collective-permute-start(bf16[8,2048]{1,0:T(8,128)(2,1)S(1)} %slice.235), channel_id=1, source_target_pairs={{0,2},{2,4},{4,6},{6,8},{8,10},{10,12},{12,14},{14,16},{16,18},{18... | collective-permute-start | bytes 98312 | tf_op jit(solution)/shard_map/ppermute | solution.py:21
  36.4 169.7 %all-gather.7.cloned.1.call-done = bf16[2048,3712]{1,0:T(8,128)(2,1)} async-done(((bf16[128,3712]{1,0:T(8,128)(2,1)}), bf16[2048,3712]{1,0:T(8,128)(2,1)}) %all-gather.7.cloned.1.call-update) | async-done | bytes 15204368 | tf_op jit(solution)/shard_map/all_gather | solution.py:204
  206.1 8.4 %fusion.12 = bf16[264,3072]{1,0:T(8,128)(2,1)S(1)} fusion(bf16[2048,3712]{1,0:T(8,128)(2,1)} %all-gather.7.cloned.1.call-done, bf16[256,2048]{1,0:T(8,128)(2,1)} %all-gather.5.cloned.1.call-done, bf16[8,2048]{1,0:T(8,128)(2,1)S(1)} %collective-permute-done), kind=kOutput, calls=%fused_computation.18 | convolution fusion | flops 3324862464 | bytes 15286272 | tf_op jit(solution)/shard_map/dot_general | solution.py:208
  217.7 2.1 copy.64
  219.7 4.1 %fusion.71 = (bf16[32,4,8,128]{3,2,1,0:T(8,128)(2,1)}, bf16[32,4,8,128]{3,2,1,0:T(8,128)(2,1)S(1)}) fusion(f32[259,512]{1,0:T(8,128)} %get-tuple-element.36, f32[512]{0:T(512)S(1)} %bitcast.121, f32[512]{0:T(512)S(1)} %bitcast.122, f32[512]{0:T(512)S(1)} %bitcast.120, f32[512]{0:T(512)S(1)} %bitcast.119, f32[259,512]{1,0:T(8,128)} %get-tuple-element.37, ...), kind=kLoop, calls=%fused_computation.105 | loop fusion | flops 3145728 | bytes 4734976
  228.3 2.2 convolution_convert_fusion.2
  235.5 3.5 %slice.232 = bf16[2048,640]{1,0:T(8,128)(2,1)} slice(bf16[2048,3712]{1,0:T(8,128)(2,1)} %all-gather.7.cloned.1.call-done), slice={[0:2048], [3072:3712]} | slice | bytes 5242880 | tf_op jit(solution)/shard_map/slice | solution.py:207
  239.0 4.5 %reshape.324 = bf16[4096,320]{1,0:T(8,128)(2,1)S(1)} reshape(bf16[2048,640]{1,0:T(8,128)(2,1)} %slice.232) | data formatting | bytes 5242880 | tf_op jit(solution)/shard_map/reshape | solution.py:207
  244.6 2.3 copy.61
  247.0 2.4 convolution_convert_fusion.1
  249.7 7.9 %fusion = (f32[4,256]{1,0:T(4,128)S(1)}, f32[4,256,4096]{2,1,0:T(8,128)}) fusion(pred[256,4096]{1,0:T(8,128)(4,1)S(1)} %copy-done.4, bf16[4096,4,64]{0,2,1:T(8,128)(2,1)S(1)} %broadcast_in_dim.57, bf16[4096,4,128]{0,2,1:T(8,128)(2,1)S(1)} %bitcast.96, bf16[256,4,32]{0,2,1:T(8,128)(2,1)S(1)} %copy-done.19, bf16[256,4,32]{0,2,1:T(8,128)(2,1)S(1)} %copy-done.18, ...), kind=kOutput, calls=%fused_computation.2 | convolution fusion | flops 1636957184 | bytes 24514560 | tf_op jit(solution)/shard_map/qhd,khd->hqk/dot_general | solution.py:142
  257.6 3.3 %convolution_convert_fusion = bf16[4096,512]{0,1:T(8,128)(2,1)} fusion(bf16[256,512]{1,0:T(8,128)(2,1)S(1)} %copy-done.14, bf16[4096,320]{1,0:T(8,128)(2,1)S(1)} %reshape.324), kind=kOutput, calls=%fused_computation.14 | convolution fusion | flops 1075838976 | bytes 6553600 | tf_op jit(solution)/shard_map/dot_general | solution.py:133
  260.9 8.4 %fusion.1 = f32[4,256]{1,0:T(4,128)S(1)} fusion(f32[4,256,4096]{2,1,0:T(8,128)} %get-tuple-element.64, f32[4,256]{1,0:T(4,128)S(1)} %broadcast_maximum_fusion, pred[256,4096]{1,0:T(8,128)(4,1)S(1)} %copy-done.4), kind=kLoop, calls=%fused_computation.3 | loop fusion | flops 16776192 | bytes 17833984 | tf_op jit(solution)/shard_map/reduce_sum | solution.py:150
  269.3 2.3 copy-done.2
  271.6 6.8 %fusion.52 = bf16[256,4,128]{0,2,1:T(8,128)(2,1)S(1)} fusion(bf16[4096,4,128]{0,2,1:T(8,128)(2,1)} %bitcast.97, f32[4,256,4096]{2,1,0:T(8,128)S(1)} %copy-done.2, f32[4,256]{1,0:T(4,128)S(1)} %broadcast_maximum_fusion, pred[256,4096]{1,0:T(8,128)(4,1)S(1)} %copy-done.4, f32[256,4]{0,1:T(4,128)S(1)} %bitcast.123), kind=kOutput, calls=%fused_computation.67 | convolution fusion | flops 1090781184 | bytes 22290432 | tf_op jit(solution)/shard_map/hqk,khd->hqd/dot_general | solution.py:151
  279.6 2.3 fusion.30
  281.9 17.9 %all-gather.9.cloned.1.call-done = bf16[16640,128]{1,0:T(8,128)(2,1)} async-done(((bf16[1040,128]{1,0:T(8,128)(2,1)}), bf16[16640,128]{1,0:T(8,128)(2,1)}) %all-gather.9.cloned.1.call-update) | async-done | bytes 4259856 | tf_op jit(solution)/shard_map/all_gather | solution.py:89
  301.1 4.5 %multiply_reduce_fusion = bf16[1024,128]{1,0:T(8,128)(2,1)S(1)} fusion(bf16[16,1040,128]{2,1,0:T(8,128)(2,1)} %bitcast.102, f32[16,1024]{1,0:T(8,128)S(1)} %mul.480), kind=kLoop, calls=%fused_computation.7 | loop fusion | flops 6160384 | bytes 4521984 | tf_op jit(solution)/shard_map/reduce_sum | solution.py:100
  308.8 2.6 copy.67
  311.4 2.8 multiply_convert_fusion.4
  (144 shorter events, 35.4 us)
Async XLA Ops:
  7.2 221.1 %copy-start = (bf16[2048,768]{1,0:T(8,128)(2,1)S(1)}, bf16[2048,768]{1,0:T(8,128)(2,1)}, u32[]{:S(2)}) copy-start(bf16[2048,768]{1,0:T(8,128)(2,1)} %param.26) | copy-start | bytes 9437188
  7.2 10.3 %copy-start.15 = (bf16[128,1024]{1,0:T(8,128)(2,1)S(1)}, bf16[128,1024]{1,0:T(8,128)(2,1)}, u32[]{:S(2)}) copy-start(bf16[128,1024]{1,0:T(8,128)(2,1)} %param.33) | copy-start | bytes 786436
  7.2 11.0 %copy-start.17 = (bf16[128,512]{1,0:T(8,128)(2,1)S(1)}, bf16[128,512]{1,0:T(8,128)(2,1)}, u32[]{:S(2)}) copy-start(bf16[128,512]{1,0:T(8,128)(2,1)} %param.34) | copy-start | bytes 393220
  7.2 15.4 %all-gather.5.cloned.1.call-start = ((), (), s32[]{:S(2)}) async-start(), calls=%async_computation | async-start | bytes 1572864 | tf_op jit(solution)/shard_map/all_gather | solution.py:180
  10.7 195.4 %all-gather.7.cloned.1.call-start = ((), (), s32[]{:S(2)}) async-start(), calls=%async_computation.1 | async-start | bytes 16154624 | tf_op jit(solution)/shard_map/all_gather | solution.py:204
  18.2 7.7 %copy-start.33 = (f32[256]{0:T(256)S(1)}, f32[256]{0:T(256)}, u32[]{:S(2)}) copy-start(f32[256]{0:T(256)} %fusion.81) | copy-start | bytes 3076
  18.2 7.7 %copy-start.34 = (f32[32]{0:T(128)S(1)}, f32[32]{0:T(128)}, u32[]{:S(2)}) copy-start(f32[32]{0:T(128)} %multiply_power_fusion) | copy-start | bytes 388
  20.4 9.6 %copy-start.26 = (bf16[4,512]{1,0:T(4,128)(2,1)S(1)}, bf16[4,512]{1,0:T(4,128)(2,1)}, u32[]{:S(2)}) copy-start(bf16[4,512]{1,0:T(4,128)(2,1)} %param.38) | copy-start | bytes 12292
  20.5 9.6 %copy-start.27 = (bf16[4,512]{1,0:T(4,128)(2,1)S(1)}, bf16[4,512]{1,0:T(4,128)(2,1)}, u32[]{:S(2)}) copy-start(bf16[4,512]{1,0:T(4,128)(2,1)} %param.39) | copy-start | bytes 12292
  20.5 9.6 %copy-start.25 = (bf16[4,1024]{1,0:T(4,128)(2,1)S(1)}, bf16[4,1024]{1,0:T(4,128)(2,1)}, u32[]{:S(2)}) copy-start(bf16[4,1024]{1,0:T(4,128)(2,1)} %param.37) | copy-start | bytes 24580
  28.6 271.2 %all-gather.9.cloned.1.call-start = ((), (), s32[]{:S(2)}) async-start(), calls=%async_computation.2 | async-start | bytes 4526080 | tf_op jit(solution)/shard_map/all_gather | solution.py:89
  30.8 5.5 %collective-permute-start = (bf16[8,2048]{1,0:T(8,128)(2,1)S(1)}, bf16[8,2048]{1,0:T(8,128)(2,1)S(1)}, u32[]{:S(2)}, u32[]{:S(2)}) collective-permute-start(bf16[8,2048]{1,0:T(8,128)(2,1)S(1)} %slice.235), channel_id=1, source_target_pairs={{0,2},{2,4},{4,6},{6,8},{8,10},{10,12},{12,14},{14,16},{16,18},{18... | collective-permute-start | bytes 98312 | tf_op jit(solution)/shard_map/ppermute | solution.py:21
  35.3 179.2 %copy-start.21 = (f32[4,4,256]{2,1,0:T(4,128)}, f32[4,4,256]{2,1,0:T(4,128)S(1)}, u32[]{:S(2)}) copy-start(f32[4,4,256]{2,1,0:T(4,128)S(1)} %mul.456) | copy-start | bytes 49156
  35.7 178.9 %copy-start.23 = (f32[4,4,256]{2,1,0:T(4,128)}, f32[4,4,256]{2,1,0:T(4,128)S(1)}, u32[]{:S(2)}) copy-start(f32[4,4,256]{2,1,0:T(4,128)S(1)} %fusion.68) | copy-start | bytes 49156
  249.7 7.9 %copy-start.14 = (bf16[256,512]{1,0:T(8,128)(2,1)S(1)}, bf16[256,512]{1,0:T(8,128)(2,1)}, u32[]{:S(2)}) copy-start(bf16[256,512]{1,0:T(8,128)(2,1)} %param.31) | copy-start | bytes 786436
  260.9 10.7 %copy-start.2 = (f32[4,256,4096]{2,1,0:T(8,128)S(1)}, f32[4,256,4096]{2,1,0:T(8,128)}, u32[]{:S(2)}) copy-start(f32[4,256,4096]{2,1,0:T(8,128)} %get-tuple-element.64) | copy-start | bytes 50331652
  271.6 7.9 %copy-start.10 = (bf16[256,1024]{0,1:T(8,128)(2,1)S(1)}, bf16[256,1024]{0,1:T(8,128)(2,1)}, u32[]{:S(2)}) copy-start(bf16[256,1024]{0,1:T(8,128)(2,1)} %copy.64) | copy-start | bytes 1572868
  271.6 7.9 %copy-start.20 = (pred[256,256]{1,0:T(8,128)(4,1)S(1)}, pred[256,256]{1,0:T(8,128)(4,1)}, u32[]{:S(2)}) copy-start(pred[256,256]{1,0:T(8,128)(4,1)} %iota_compare_fusion.1) | copy-start | bytes 196612
  271.6 8.0 %copy-start.22 = (f32[4,4,256]{2,1,0:T(4,128)S(1)}, f32[4,4,256]{2,1,0:T(4,128)}, u32[]{:S(2)}) copy-start(f32[4,4,256]{2,1,0:T(4,128)} %copy-done.21) | copy-start | bytes 49156
  271.6 8.0 %copy-start.24 = (f32[4,4,256]{2,1,0:T(4,128)S(1)}, f32[4,4,256]{2,1,0:T(4,128)}, u32[]{:S(2)}) copy-start(f32[4,4,256]{2,1,0:T(4,128)} %copy-done.23) | copy-start | bytes 49156
  279.6 21.1 %copy-start.28 = (pred[16,16]{1,0:T(8,128)(4,1)S(1)}, pred[16,16]{1,0:T(8,128)(4,1)}, u32[]{:S(2)}) copy-start(pred[16,16]{1,0:T(8,128)(4,1)} %fusion.79) | copy-start | bytes 772
  279.6 21.2 %copy-start.32 = (pred[16]{0:T(512)(128)(4,1)S(1)}, pred[16]{0:T(512)(128)(4,1)}, u32[]{:S(2)}) copy-start(pred[16]{0:T(512)(128)(4,1)} %copy-done.31) | copy-start | bytes 52
  281.9 23.8 %copy-start.29 = (f32[4,4]{1,0:T(4,128)S(1)}, f32[4,4]{1,0:T(4,128)}, u32[]{:S(2)}) copy-start(f32[4,4]{1,0:T(4,128)} %mul.485) | copy-start | bytes 196
  281.9 25.1 %copy-start.5 = (f32[256,1024]{0,1:T(8,128)S(1)}, f32[256,1024]{0,1:T(8,128)}, u32[]{:S(2)}) copy-start(f32[256,1024]{0,1:T(8,128)} %copy.68) | copy-start | bytes 3145732
  (16 other events, 60.8 us)
Sparse Core Ops, SparseCore 0:
  10.8 11.7 all-gather.4
  28.7 177.3 all-gather.6
  225.4 74.3 all-gather.8

commit v2 on v1

--- a/solution.py
+++ b/solution.py
@@ -1,6 +1,8 @@
 import jax
 import jax.numpy as jnp
 from jax import lax
+from jax.experimental import pallas as pl
+from jax.experimental.pallas import tpu as pltpu
 from jax.sharding import PartitionSpec as P
 
 UNROTATED_WIDTH = 128
@@ -78,27 +80,167 @@
     return running, state, within
 
 
-def state_before(state, total, axis):
-    groups, per_group, dim, entries = state.shape
-    count = groups * per_group
-    flat = state.reshape(count * dim, entries).astype(jnp.bfloat16)
-    high = total.reshape(count).astype(jnp.bfloat16)
-    low = (total.reshape(count) - high.astype(jnp.float32)).astype(jnp.bfloat16)
-    tail = jnp.zeros((16, entries), jnp.bfloat16)
-    tail = tail.at[0, :count].set(high).at[1, :count].set(low)
-    everything = lax.all_gather(jnp.concatenate([flat, tail], axis=0), axis)
-    here = lax.axis_index(axis)
-    devices = everything.shape[0]
-    states = everything[:, : count * dim].reshape(devices, count, dim, entries)
-    totals = everything[:, count * dim, :count].astype(jnp.float32) + everything[
-        :, count * dim + 1, :count
-    ].astype(jnp.float32)
-    index = jnp.arange(devices)
-    between = (index[None, :] > index[:, None]) & (index[None, :] < here)
-    path = jnp.sum(jnp.where(between[:, :, None], totals[None], 0.0), axis=1)
-    factor = jnp.where((index < here)[:, None], jnp.exp(path), 0.0)
-    before = jnp.sum(states.astype(jnp.float32) * factor[:, :, None, None], axis=0)
-    return before.reshape(state.shape)
+def exchange(items, plane, name, number):
+    devices, cores = lax.axis_size("sp"), lax.axis_size("tp")
+    planes = devices // plane
+    counts = [{"plane": plane, "line": planes, "all": devices}[item[1]] for item in items]
+    amount = len(items)
+    starts = [sum(counts[:i]) for i in range(amount)]
+    whole = any(item[1] == "all" for item in items)
+    shared = any(item[2] for item in items)
+
+    def kernel(*refs):
+        ins, outs = refs[:amount], refs[amount : 2 * amount]
+        send, recv, pass_send, pass_recv, own = refs[2 * amount :]
+        here, core = lax.axis_index("sp"), lax.axis_index("tp")
+        across, within = here // plane, here % plane
+
+        def place(reach, step):
+            if reach == "plane":
+                slot = (within + step + plane) % plane
+                return across * plane + slot, slot
+            if reach == "line":
+                slot = (across + step + planes) % planes
+                return slot * plane + within, slot
+            slot = (here + step + devices) % devices
+            return slot, slot
+
+        barrier = pltpu.get_barrier_semaphore()
+        greeted = 0
+        for reach in ("plane", "line", "all"):
+            if reach == "all" and not whole or reach != "all" and whole:
+                continue
+            if not any(item[1] == reach for item in items):
+                continue
+            size = {"plane": plane, "line": planes, "all": devices}[reach]
+            for step in range(1, size):
+                pl.semaphore_signal(
+                    barrier,
+                    inc=1,
+                    device_id=(place(reach, step)[0], core),
+                    device_id_type=pl.DeviceIdType.MESH,
+                )
+                greeted += 1
+        if shared:
+            for turn in range(1, cores):
+                pl.semaphore_signal(
+                    barrier,
+                    inc=1,
+                    device_id=(here, (core + turn) % cores),
+                    device_id_type=pl.DeviceIdType.MESH,
+                )
+                greeted += 1
+        pl.semaphore_wait(barrier, greeted)
+
+        def target(i, slot, who):
+            return outs[i].at[slot, who] if items[i][2] else outs[i].at[slot]
+
+        def sent(i, step):
+            goal, goal_slot = place(items[i][1], step)
+            mine = place(items[i][1], 0)[1]
+            return pltpu.make_async_remote_copy(
+                src_ref=ins[i].at[goal_slot] if items[i][3] else ins[i],
+                dst_ref=target(i, mine, core),
+                send_sem=send.at[starts[i] + step],
+                recv_sem=recv.at[starts[i] + step],
+                device_id=(goal, core),
+                device_id_type=pl.DeviceIdType.MESH,
+            )
+
+        def arrived(i, step):
+            slot = place(items[i][1], -step)[1]
+            return pltpu.make_async_remote_copy(
+                src_ref=ins[i].at[slot] if items[i][3] else ins[i],
+                dst_ref=target(i, slot, core),
+                send_sem=send.at[starts[i] + step],
+                recv_sem=recv.at[starts[i] + step],
+                device_id=(here, core),
+                device_id_type=pl.DeviceIdType.MESH,
+            )
+
+        def passed(i, step, turn, outgoing):
+            slot = place(items[i][1], -step)[1]
+            other = (core + turn) % cores
+            owner = core if outgoing else (core - turn + cores) % cores
+            return pltpu.make_async_remote_copy(
+                src_ref=ins[i] if step == 0 else target(i, slot, core),
+                dst_ref=target(i, slot, owner),
+                send_sem=pass_send.at[(starts[i] + step) * cores + turn],
+                recv_sem=pass_recv.at[(starts[i] + step) * cores + turn],
+                device_id=(here, other),
+                device_id_type=pl.DeviceIdType.MESH,
+            )
+
+        kept = []
+        for i in range(amount):
+            for step in range(1, counts[i]):
+                sent(i, step).start()
+        for i in range(amount):
+            slot = place(items[i][1], 0)[1]
+            local = pltpu.make_async_copy(
+                ins[i].at[slot] if items[i][3] else ins[i], target(i, slot, core), own.at[i]
+            )
+            local.start()
+            kept.append(local)
+            if items[i][2]:
+                for turn in range(1, cores):
+                    passed(i, 0, turn, True).start()
+        for i in range(amount):
+            for step in range(1, counts[i]):
+                arrived(i, step).wait_recv()
+                if items[i][2]:
+                    for turn in range(1, cores):
+                        passed(i, step, turn, True).start()
+        for i in range(amount):
+            kept[i].wait()
+            for step in range(counts[i]):
+                if step > 0:
+                    sent(i, step).wait_send()
+                if items[i][2]:
+                    for turn in range(1, cores):
+                        passed(i, step, turn, True).wait_send()
+                        passed(i, step, turn, False).wait_recv()
+
+    shapes = []
+    for (array, reach, over, selected), count in zip(items, counts):
+        lead = (count, cores) if over else (count,)
+        tail = array.shape[1:] if selected else array.shape
+        shapes.append(jax.ShapeDtypeStruct(lead + tail, array.dtype))
+    slots = sum(counts)
+    return pl.pallas_call(
+        kernel,
+        out_shape=shapes,
+        in_specs=[pl.BlockSpec(memory_space=pltpu.VMEM)] * amount,
+        out_specs=[pl.BlockSpec(memory_space=pl.ANY)] * amount,
+        scratch_shapes=[
+            pltpu.SemaphoreType.DMA((slots,)),
+            pltpu.SemaphoreType.DMA((slots,)),
+            pltpu.SemaphoreType.DMA((slots * cores,)),
+            pltpu.SemaphoreType.DMA((slots * cores,)),
+            pltpu.SemaphoreType.DMA((amount,)),
+        ],
+        compiler_params=pltpu.CompilerParams(
+            collective_id=number, has_side_effects=True, vmem_limit_bytes=16 * 1024 * 1024
+        ),
+        cost_estimate=pl.CostEstimate(
+            flops=10**8, bytes_accessed=4 * 2**20, transcendentals=0
+        ),
+        name=name,
+    )(*[item[0] for item in items])
+
+
+def plain_exchange(items, plane):
+    results = []
+    for array, reach, over, selected in items:
+        value = array
+        if over:
+            value = lax.all_gather(value, "tp")
+        if reach == "plane":
+            value = value if selected else value[None]
+        else:
+            value = lax.all_gather(value, "sp")
+        results.append(value)
+    return results
 
 
 def gated_norm(mixed, gate, gain):
@@ -176,81 +318,71 @@
     skip_gain,
     group_gain,
 ):
+    groups = scan_write.shape[1] // SSM_STATE
+    devices, cores = lax.axis_size("sp"), lax.axis_size("tp")
+    plane = groups if devices % groups == 0 else 1
+    planes = devices // plane
+    sp_index, core = lax.axis_index("sp"), lax.axis_index("tp")
+    across, within = sp_index // plane, sp_index % plane
+    own_groups = groups // plane
+    direct = plane > 1
+
+    def move(items, name, number):
+        return exchange(items, plane, name, number) if direct else plain_exchange(items, plane)
+
+    depth = scan_input.shape[0]
+    widths = [w.shape[1] // plane for w in (scan_input, scan_gate, scan_write, scan_read)]
+    offsets = [sum(widths[:i]) for i in range(4)]
+    packed = jnp.stack(
+        [
+            jnp.concatenate(
+                [
+                    w[:, n * size : (n + 1) * size]
+                    for w, size in zip((scan_input, scan_gate, scan_write, scan_read), widths)
+                ],
+                axis=1,
+            )
+            for n in range(plane)
+        ]
+    )
+    (part_weights,) = move([(packed, "plane", False, True)], "weights_in_plane", 1)
+    weights = lax.all_gather(
+        part_weights.reshape(plane * depth, -1),
+        "sp",
+        axis=0,
+        tiled=True,
+        axis_index_groups=[[p * plane + n for p in range(planes)] for n in range(plane)],
+    )
+
     own_normed = rms_scale(tokens, mix_gain).astype(jnp.bfloat16)
-    rows = lax.all_gather(own_normed, "tp", axis=0, tiled=True)
-    length = rows.shape[0]
-    width = tokens.shape[1]
-    sp_index = lax.axis_index("sp")
-    positions = sp_index * length + jnp.arange(length, dtype=jnp.int32)
-    heads = key_up.shape[1] // UNROTATED_WIDTH
-    local_heads = decay_log.shape[0]
+    part = tokens.shape[0]
+    length = part * cores
     latent_width = compressed_projection.shape[1]
     small = jnp.dot(
-        rows,
-        jnp.concatenate([compressed_projection, rope_proj, step_proj], axis=1),
+        own_normed,
+        jnp.concatenate([compressed_projection, rope_proj], axis=1),
         preferred_element_type=jnp.float32,
     )
     latent = rms_scale(small[:, :latent_width], compressed_norm_gain).astype(jnp.bfloat16)
-    key_turned = rotate(small[:, latent_width : latent_width + ROPE], positions).astype(
-        jnp.bfloat16
-    )
-    step_all = small[:, latent_width + ROPE :]
-    edge_rows = from_behind(rows[length - 8 :], "sp", 1)
-    keys = jnp.concatenate([latent, key_turned], axis=1)
-    depth = scan_input.shape[0]
-    packed = jnp.concatenate(
-        [scan_input, scan_gate, scan_write, scan_read, keys.reshape(depth, -1)], axis=1
-    )
-    everything = lax.all_gather(packed, "sp", axis=0, tiled=True)
-    widths = [w.shape[1] for w in (scan_input, scan_gate, scan_write, scan_read)]
-    scan_width = sum(widths)
-    all_keys = everything[:, scan_width:].reshape(-1, latent_width + ROPE)
-    projected = jnp.dot(
-        jnp.concatenate([edge_rows, rows], axis=0),
-        everything[:, :scan_width],
-        preferred_element_type=jnp.float32,
-    ).astype(jnp.bfloat16)
-    edge, projected = projected[:8], projected[8:]
-    gate = projected[:, widths[0] : widths[0] + widths[1]]
-    span = conv_input.shape[0] - 1
-
-    def convolved(start, size, taps):
-        return short_conv(
-            projected[:, start : start + size], edge[8 - span :, start : start + size], taps
-        )
-
-    head_conv = convolved(0, widths[0], conv_input)
-    writes = convolved(widths[0] + widths[1], widths[2], conv_write)
-    reads = convolved(widths[0] + widths[1] + widths[2], widths[3], conv_read)
-    step_size = jax.nn.softplus(
-        lax.dynamic_slice_in_dim(step_all, lax.axis_index("tp") * local_heads, local_heads, 1)
-    )
-    groups = scan_write.shape[1] // SSM_STATE
-    per_group = local_heads // groups
-    log_decay = -jnp.exp(decay_log)[None, :] * step_size + decay_offset
-    head_values = jnp.transpose(
-        head_conv.reshape(length, groups, per_group, SSM_DIM), (1, 2, 0, 3)
-    )
-    step_values = step_size.T.reshape(groups, per_group, length)
-    decay_values = log_decay.T.reshape(groups, per_group, length)
-    write_values = jnp.transpose(writes.reshape(length, groups, SSM_STATE), (1, 0, 2))
-    read_values = jnp.transpose(reads.reshape(length, groups, SSM_STATE), (1, 0, 2))
-    running, final_state, mixed = local_scan(
-        head_values, step_values, decay_values, write_values, read_values
-    )
-    incoming = state_before(final_state, running[..., -1], "sp")
-    carried = jnp.einsum(
-        "gln,grpn->grlp",
-        read_values,
-        incoming.astype(jnp.bfloat16),
-        preferred_element_type=jnp.float32,
-    )
-    mixed = (
-        mixed
-        + carried * jnp.exp(running)[..., None]
-        + skip_gain.reshape(groups, per_group)[:, :, None, None] * head_values.astype(jnp.float32)
-    )
-    scanned = gated_norm(jnp.transpose(mixed, (2, 0, 1, 3)), gate, group_gain)
+    part_positions = sp_index * length + core * part + jnp.arange(part, dtype=jnp.int32)
+    key_turned = rotate(small[:, latent_width:], part_positions).astype(jnp.bfloat16)
+    padding = jnp.zeros((part, -(latent_width + ROPE) % 128), jnp.bfloat16)
+    own_keys = jnp.concatenate([latent, key_turned, padding], axis=1)
+    all_keys, all_rows, offsets_seen = move(
+        [
+            (own_keys, "all", True, False),
+            (own_normed, "plane", True, False),
+            (decay_offset.T, "plane", False, False),
+        ],
+        "rows_and_keys",
+        2,
+    )
+    all_keys = all_keys.reshape(devices * length, -1)
+    all_rows = all_rows.reshape(plane * length, -1)
+    edge_rows = from_behind(all_rows[plane * length - 8 :], "sp", plane)
+    positions = sp_index * length + jnp.arange(length, dtype=jnp.int32)
+    rows = lax.dynamic_slice_in_dim(all_rows, within * length, length, 0)
+    heads = key_up.shape[1] // UNROTATED_WIDTH
 
     query = jnp.dot(rows, query_proj, preferred_element_type=jnp.float32).astype(jnp.bfloat16)
     query = query.reshape(length, heads, UNROTATED_WIDTH + ROPE)
@@ -270,7 +402,7 @@
         query_turned,
         positions,
         all_keys[:, :latent_width],
-        all_keys[:, latent_width:],
+        all_keys[:, latent_width : latent_width + ROPE],
         key_positions,
         key_up,
         value_up_weight,
@@ -278,6 +410,109 @@
     attended = jnp.transpose((summed / total[..., None]).astype(jnp.bfloat16), (1, 0, 2)).reshape(
         length, heads * VALUE_WIDTH
     )
+
+    def own_part(array, axis, size):
+        return lax.dynamic_slice_in_dim(array, within * size, size, axis)
+
+    local_heads = decay_log.shape[0]
+    own_heads = local_heads // plane
+    per_group = local_heads // groups
+    step_raw = jnp.dot(
+        all_rows,
+        lax.dynamic_slice_in_dim(
+            step_proj, core * local_heads + within * own_heads, own_heads, 1
+        ),
+        preferred_element_type=jnp.float32,
+    )
+    step_size = jax.nn.softplus(step_raw)
+    own_offset = own_part(offsets_seen, 1, own_heads)
+    step_values = jnp.transpose(step_size.reshape(plane, length, own_heads), (0, 2, 1))
+    decay_values = (
+        -jnp.exp(own_part(decay_log, 0, own_heads))[None, :, None] * step_values + own_offset
+    )
+
+    projected = jnp.dot(all_rows, weights, preferred_element_type=jnp.float32).astype(jnp.bfloat16)
+    edge = jnp.dot(edge_rows, weights, preferred_element_type=jnp.float32).astype(jnp.bfloat16)
+    span = conv_input.shape[0] - 1
+
+    def convolved(i, taps):
+        at = slice(offsets[i], offsets[i] + widths[i])
+        return short_conv(projected[:, at], edge[8 - span :, at], own_part(taps, 1, widths[i]))
+
+    head_conv = convolved(0, conv_input)
+    gate = projected[:, offsets[1] : offsets[1] + widths[1]]
+    writes = convolved(2, conv_write)
+    reads = convolved(3, conv_read)
+    blocks = plane * own_groups
+
+    def by_block(values, last):
+        split = values.reshape(plane, length, own_groups, last)
+        return jnp.transpose(split, (0, 2, 1, 3)).reshape(blocks, length, last)
+
+    head_values = jnp.transpose(
+        head_conv.reshape(plane, length, own_groups, per_group, SSM_DIM), (0, 2, 3, 1, 4)
+    ).reshape(blocks, per_group, length, SSM_DIM)
+    write_values = by_block(writes, SSM_STATE)
+    read_values = by_block(reads, SSM_STATE)
+    running, state, mixed = local_scan(
+        head_values,
+        step_values.reshape(blocks, per_group, length),
+        decay_values.reshape(blocks, per_group, length),
+        write_values,
+        read_values,
+    )
+    states = state.reshape(plane, own_heads, SSM_DIM, SSM_STATE)
+    totals = running[..., -1].reshape(plane, own_heads)
+    before, decayed = [jnp.zeros_like(states[0])], [jnp.zeros_like(totals[0])]
+    for index in range(plane):
+        before.append(jnp.exp(totals[index])[:, None, None] * before[-1] + states[index])
+        decayed.append(totals[index] + decayed[-1])
+    sent_total = jnp.pad(decayed[-1][None, :], ((0, 7), (0, 128 - own_heads)))
+    seen_states, seen_totals = move(
+        [
+            (before[-1].reshape(-1, SSM_STATE).astype(jnp.bfloat16), "line", False, False),
+            (sent_total, "line", False, False),
+        ],
+        "states",
+        3,
+    )
+    seen_states = seen_states.reshape(planes, own_heads, SSM_DIM, SSM_STATE).astype(jnp.float32)
+    seen_totals = seen_totals[:, 0, :own_heads]
+    index = jnp.arange(planes)
+    between = (index[None, :] > index[:, None]) & (index[None, :] < across)
+    path = jnp.sum(jnp.where(between[:, :, None], seen_totals[None], 0.0), axis=1)
+    reached = (index < across)[:, None]
+    factor = jnp.where(reached, jnp.exp(path), 0.0)
+    incoming = jnp.sum(seen_states * factor[:, :, None, None], axis=0)
+    entered = jnp.stack(
+        [
+            before[k] + jnp.exp(decayed[k])[:, None, None] * incoming
+            for k in range(plane)
+        ]
+    ).reshape(blocks, per_group, SSM_DIM, SSM_STATE)
+    carried = jnp.einsum(
+        "gln,grpn->grlp",
+        read_values,
+        entered.astype(jnp.bfloat16),
+        preferred_element_type=jnp.float32,
+    )
+    skip = jnp.broadcast_to(
+        own_part(skip_gain, 0, own_heads).reshape(1, own_groups, per_group),
+        (plane, own_groups, per_group),
+    ).reshape(blocks, per_group, 1, 1)
+    mixed = (
+        mixed
+        + carried * jnp.exp(running)[..., None]
+        + skip * head_values.astype(jnp.float32)
+    )
+    mixed = jnp.transpose(
+        mixed.reshape(plane, own_groups, per_group, length, SSM_DIM), (0, 3, 1, 2, 4)
+    ).reshape(plane * length, own_groups, per_group, SSM_DIM)
+    scanned = gated_norm(mixed, gate, own_part(group_gain, 0, widths[0]))
+    (columns,) = move(
+        [(scanned.reshape(plane, length, -1), "plane", False, True)], "outputs_in_plane", 4
+    )
+    scanned = jnp.transpose(columns, (1, 0, 2)).reshape(length, -1)
     return (attended, scanned)
 
 

time: 322 us -> 242 us (0.75)
  waiting for transfers between devices: 190 us -> 0.04 us
  Pallas kernels: 0 us -> 94.1 us
  starting transfers between devices: 3.75 us -> 27.3 us
  other arithmetic: 37.4 us -> 24.1 us
  matrix products: 37.7 us -> 41.5 us
    all_gather x3 -> x1, waiting for transfers between devices: 190 us -> 0.02 us  [shards(): lax.all_gather(part_weights.reshape(plane * depth, -1), 'sp', axis=0, til...]
    pallas_call x0 -> x4, Pallas kernels: none -> 94.1 us  [exchange(): pl.pallas_call(kernel, out_shape=shapes, in_specs=[pl.BlockSpec(memory_sp...]
    ppermute x1, starting transfers between devices: 3.63 us -> 27.3 us  [from_behind(): lax.ppermute(value, axis, [(source, source + steps) for source in range(i...]
    reshape x4 -> x2, local copies, waits for them, and re-layouts: 7.28 us -> 0.97 us  [shards(): head_conv.reshape(plane, length, own_groups, per_group, SSM_DIM)]
    another operation x1 -> x2, local copies, waits for them, and re-layouts: 0.09 us -> 5.12 us  [gated_norm(): flat = mixed.reshape(length, groups, -1)]
    reduce_sum x2, other arithmetic: 4.64 us -> 0.3 us  [the longest x1 0.21 us: shards(): incoming = jnp.sum(seen_states * factor[:, :, None, None], axis=0)]
    unnamed x1 -> x0, other arithmetic: 4.14 us -> none
    unnamed x80 -> x75, local copies, waits for them, and re-layouts: 14.6 us -> 12 us
  transfers between devices with their start and end apart: 4 -> 2, of which waited for: 3 -> 0; matrix products, arithmetic and copies ran while one was open for 21% -> 30% of each run, Pallas kernels for 0% -> 24%
where the time goes in v2:
time: 242 us; the launch traced here: 241 us
  Pallas kernels  94.1 us (39%)
  matrix products  41.5 us (17%)
  local copies, waits for them, and re-layouts  39 us (16%)
  starting transfers between devices  27.3 us (11%)
  other arithmetic  24.1 us (10%)
  between operations  14.8 us (6%)
    pallas_call x4, Pallas kernels, exchange(): pl.pallas_call(kernel, out_shape=shapes, in_specs=[pl.BlockSpec(memory_sp...  94.1 us
    ppermute x1, starting transfers between devices, from_behind(): lax.ppermute(value, axis, [(source, source + steps) for source in range(i...  27.3 us
    unnamed x75, local copies, waits for them, and re-layouts  12 us
    dot_general x1, matrix products, attend_piece(): jnp.einsum('qhd,khd->hqk', query_whole, key_whole, preferred_element_type...  9.48 us
    reduce_sum x1, other arithmetic, attend_piece(): total = jnp.sum(weights, axis=-1)  8.57 us
    dot_general x1, matrix products, shards(): jnp.dot(all_rows, weights, preferred_element_type=jnp.float32)  6.71 us
    dot_general x1, matrix products, attend_piece(): jnp.einsum('hqk,khd->hqd', weights.astype(jnp.bfloat16), values, preferre...  6.7 us
    another operation x2, local copies, waits for them, and re-layouts, gated_norm(): flat = mixed.reshape(length, groups, -1)  5.12 us
  transfers between devices with their start and end apart: 2, of which 0 were waited for; matrix products, arithmetic and copies ran while one was open for 30% of the time, Pallas kernels for 24%

profile of v2, /device:TPU:0, one launch (start us, length us, event | category | flops | bytes accessed | tf_op | source)
XLA Modules:
  0.0 240.8 jit_solution(7208077325304112949)
XLA Ops:
  11.2 13.6 %weights_in_plane.1 = bf16[4,128,768]{2,1,0:T(8,128)(2,1)S(1)} custom-call(bf16[4,128,768]{2,1,0:T(8,128)(2,1)S(1)} %pad_maximum_fusion.refs_0_), custom_call_target="tpu_custom_call" | custom-call | flops 100000000 | bytes 4194304 | tf_op jit(solution)/shard_map/weights_in_plane/pallas_call | solution.py:210
  29.3 1.8 fusion.19
  31.8 57.7 %rows_and_keys.1 = (bf16[16,2,128,384]{3,2,1,0:T(8,128)(2,1)S(1)}, bf16[4,2,128,2048]{3,2,1,0:T(8,128)(2,1)S(1)}, f32[4,16,256]{2,1,0:T(8,128)S(1)}) custom-call(bf16[128,384]{1,0:T(8,128)(2,1)S(1)} %maximum_maximum_fusion.refs_0_, bf16[128,2048]{1,0:T(8,128)(2,1)S(1)} %fusion.32.refs_1_, f32[16,256]{1,0:T(8,128)S(1)} %bitcast.143), custom_call_target="tpu_custom_call" | custom-call | flops 100000000 | bytes 4194304 | tf_op jit(solution)/shard_map/rows_and_keys/pallas_call | solution.py:210
  91.2 1.9 copy-done.4
  93.8 27.3 %collective-permute-start = (bf16[8,2048]{1,0:T(8,128)(2,1)}, bf16[8,2048]{1,0:T(8,128)(2,1)}, u32[]{:S(2)}, u32[]{:S(2)}) collective-permute-start(bf16[8,2048]{1,0:T(8,128)(2,1)} %slice.293), channel_id=1, source_target_pairs={{0,8},{2,10},{4,12},{6,14},{8,16},{10,18},{12,20},{14,22},{16,24},... | collective-permute-start | bytes 98312 | tf_op jit(solution)/shard_map/ppermute | solution.py:23
  121.7 3.0 %convolution_convert_fusion.3 = bf16[256,768]{1,0:T(8,128)(2,1)} fusion(bf16[2048,768]{1,0:T(8,128)(2,1)S(1)} %copy-done, bf16[1024,2048]{1,0:T(8,128)(2,1)} %bitcast.137, s32[]{:T(128)S(6)} %select_n.59), kind=kOutput, calls=%fused_computation.40 | convolution fusion | flops 805502976 | bytes 4587524 | tf_op jit(solution)/shard_map/dot_general | solution.py:387
  124.7 2.1 copy.63
  130.1 3.4 %compare_select_fusion = f32[1024,4]{0,1:T(4,128)S(1)} fusion(bf16[1024,2048]{1,0:T(8,128)(2,1)} %bitcast.138, bf16[2048,32]{0,1:T(8,128)(2,1)} %param.32, s32[]{:T(128)S(6)} %select_n.63), kind=kOutput, calls=%fused_computation.139 | convolution fusion | flops 16801792 | bytes 4227076 | tf_op jit(solution)/shard_map/dot_general | solution.py:420
  142.1 3.3 %convolution_convert_fusion.1 = bf16[4096,512]{0,1:T(8,128)(2,1)} fusion(bf16[256,512]{1,0:T(8,128)(2,1)S(1)} %copy-done.12, bf16[4096,384]{1,0:T(8,128)(2,1)S(1)} %bitcast.134), kind=kOutput, calls=%fused_computation.12 | convolution fusion | flops 1075838976 | bytes 6553600 | tf_op jit(solution)/shard_map/dot_general | solution.py:270
  145.4 2.3 copy.64
  151.4 9.5 %fusion = (f32[4,256]{1,0:T(4,128)S(1)}, f32[4,256,4096]{2,1,0:T(8,128)}) fusion(pred[256,4096]{1,0:T(8,128)(4,1)S(1)} %iota_compare_fusion, bf16[4096,4,64]{0,2,1:T(8,128)(2,1)S(1)} %broadcast_in_dim.61, bf16[4096,4,128]{0,2,1:T(8,128)(2,1)} %bitcast.144, bf16[256,4,32]{0,2,1:T(8,128)(2,1)S(1)} %get-tuple-element.37, ...), kind=kOutput, calls=%fused_computation.2 | convolution fusion | flops 1636957184 | bytes 24514560 | tf_op jit(solution)/shard_map/qhd,khd->hqk/dot_general | solution.py:284
  160.8 3.3 %convolution_convert_fusion = bf16[4096,512]{0,1:T(8,128)(2,1)} fusion(bf16[256,512]{1,0:T(8,128)(2,1)S(1)} %copy-done.13, bf16[4096,384]{1,0:T(8,128)(2,1)S(1)} %bitcast.135), kind=kOutput, calls=%fused_computation.11 | convolution fusion | flops 1075838976 | bytes 6553600 | tf_op jit(solution)/shard_map/dot_general | solution.py:275
  164.1 8.6 %fusion.1 = f32[4,256]{1,0:T(4,128)S(1)} fusion(f32[4,256,4096]{2,1,0:T(8,128)} %get-tuple-element.75, f32[4,256]{1,0:T(4,128)S(1)} %broadcast_maximum_fusion, pred[256,4096]{1,0:T(8,128)(4,1)S(1)} %iota_compare_fusion), kind=kLoop, calls=%fused_computation.3 | loop fusion | flops 16776192 | bytes 17833984 | tf_op jit(solution)/shard_map/reduce_sum | solution.py:292
  172.7 2.0 copy-done.8
  174.8 6.7 %fusion.45 = bf16[256,4,128]{0,2,1:T(8,128)(2,1)S(1)} fusion(bf16[4096,4,128]{0,2,1:T(8,128)(2,1)} %bitcast.145, f32[4,256,4096]{2,1,0:T(8,128)S(1)} %copy-done.8, f32[4,256]{1,0:T(4,128)S(1)} %broadcast_maximum_fusion, pred[256,4096]{1,0:T(8,128)(4,1)S(1)} %iota_compare_fusion, f32[256,4]{0,1:T(4,128)S(1)} %bitcast.164), kind=kOutput, calls=%fused_computation.63 | convolution fusion | flops 1090781184 | bytes 22290432 | tf_op jit(solution)/shard_map/hqk,khd->hqd/dot_general | solution.py:293
  183.5 6.7 %convolution_convert_fusion.2 = bf16[1024,768]{1,0:T(8,128)(2,1)S(1)} fusion(bf16[1024,2048]{1,0:T(8,128)(2,1)} %bitcast.139, bf16[2048,768]{1,0:T(8,128)(2,1)} %all-gather.2.cloned.1.call-done), kind=kOutput, calls=%fused_computation.24 | convolution fusion | flops 3222011904 | bytes 8912896 | tf_op jit(solution)/shard_map/dot_general | solution.py:434
  194.5 8.9 %states.1 = (bf16[4,256,128]{2,1,0:T(8,128)(2,1)S(1)}, f32[4,8,128]{2,1,0:T(8,128)S(1)}) custom-call(bf16[256,128]{1,0:T(8,128)(2,1)S(1)} %fusion.74.refs_0_, f32[8,128]{1,0:T(8,128)S(1)} %pad.4.refs_1_), custom_call_target="tpu_custom_call" | custom-call | flops 100000000 | bytes 4194304 | tf_op jit(solution)/shard_map/states/pallas_call | solution.py:210
  206.5 1.8 copy.77
  208.2 3.3 %reshape.418 = f32[1024,256]{1,0:T(8,128)} reshape(f32[4,256,1,4,64]{4,3,1,0,2:T(4,128)} %copy.77) | data formatting | bytes 2097152 | tf_op jit(solution)/shard_map/reshape;reshape | solution.py:249
  211.6 1.8 multiply_reduce_fusion
  213.4 1.7 multiply_convert_fusion.2
  215.1 13.9 %outputs_in_plane.1 = bf16[4,256,256]{2,1,0:T(8,128)(2,1)S(1)} custom-call(bf16[4,256,256]{2,1,0:T(8,128)(2,1)S(1)} %bitcast.142), custom_call_target="tpu_custom_call" | custom-call | flops 100000000 | bytes 4194304 | tf_op jit(solution)/shard_map/outputs_in_plane/pallas_call | solution.py:210
  229.8 2.1 copy.69
  231.9 2.0 copy.71
  (157 shorter events, 37.3 us)
Async XLA Ops:
  7.2 114.5 %copy-start = (bf16[2048,768]{1,0:T(8,128)(2,1)S(1)}, bf16[2048,768]{1,0:T(8,128)(2,1)}, u32[]{:S(2)}) copy-start(bf16[2048,768]{1,0:T(8,128)(2,1)} %param.22) | copy-start | bytes 9437188
  7.2 19.8 %copy-start.11 = (bf16[2048,64]{0,1:T(8,128)(2,1)S(1)}, bf16[2048,64]{0,1:T(8,128)(2,1)}, u32[]{:S(2)}) copy-start(bf16[2048,64]{0,1:T(8,128)(2,1)} %param.25) | copy-start | bytes 786436
  7.2 20.8 %copy-start.18 = (f32[2048]{0:T(1024)S(1)}, f32[2048]{0:T(1024)}, u32[]{:S(2)}) copy-start(f32[2048]{0:T(1024)} %param.21) | copy-start | bytes 24580
  7.2 176.3 %all-gather.2.cloned.1.call-start = ((), (), s32[]{:S(2)}) async-start(), calls=%async_computation | async-start | bytes 3932160 | tf_op jit(solution)/shard_map/all_gather | solution.py:349
  11.2 20.4 %copy-start.32 = (f32[256]{0:T(256)S(1)}, f32[256]{0:T(256)}, u32[]{:S(2)}) copy-start(f32[256]{0:T(256)} %param.24) | copy-start | bytes 3076
  11.2 20.6 %copy-start.7 = (f32[256,16]{0,1:T(8,128)S(1)}, f32[256,16]{0,1:T(8,128)}, u32[]{:S(2)}) copy-start(f32[256,16]{0,1:T(8,128)} %param.37) | copy-start | bytes 49156
  93.8 96.5 %collective-permute-start = (bf16[8,2048]{1,0:T(8,128)(2,1)}, bf16[8,2048]{1,0:T(8,128)(2,1)}, u32[]{:S(2)}, u32[]{:S(2)}) collective-permute-start(bf16[8,2048]{1,0:T(8,128)(2,1)} %slice.293), channel_id=1, source_target_pairs={{0,8},{2,10},{4,12},{6,14},{8,16},{10,18},{12,20},{14,22},{16,24},... | collective-permute-start | bytes 98312 | tf_op jit(solution)/shard_map/ppermute | solution.py:23
  124.7 8.9 %copy-start.34 = (f32[16]{0:T(128)S(1)}, f32[16]{0:T(128)}, u32[]{:S(2)}) copy-start(f32[16]{0:T(128)} %param.36) | copy-start | bytes 196
  124.7 13.6 %copy-start.35 = (f32[16]{0:T(128)S(1)}, f32[16]{0:T(128)}, u32[]{:S(2)}) copy-start(f32[16]{0:T(128)} %param.38) | copy-start | bytes 196
  124.7 16.4 %copy-start.3 = (bf16[16,2,128,384]{3,2,1,0:T(8,128)(2,1)S(1)}, bf16[16,2,128,384]{3,2,1,0:T(8,128)(2,1)}, u32[]{:S(2)}) copy-start(bf16[16,2,128,384]{3,2,1,0:T(8,128)(2,1)} %copy-done.2) | copy-start | bytes 9437188
  128.4 13.7 %copy-start.12 = (bf16[256,512]{1,0:T(8,128)(2,1)S(1)}, bf16[256,512]{1,0:T(8,128)(2,1)}, u32[]{:S(2)}) copy-start(bf16[256,512]{1,0:T(8,128)(2,1)} %param.26) | copy-start | bytes 786436
  133.5 11.9 %copy-start.14 = (f32[1024,4]{0,1:T(4,128)}, f32[1024,4]{0,1:T(4,128)S(1)}, u32[]{:S(2)}) copy-start(f32[1024,4]{0,1:T(4,128)S(1)} %compare_select_fusion) | copy-start | bytes 49156
  135.3 10.0 %copy-start.28 = (f32[4]{0:T(128)}, f32[4]{0:T(128)S(1)}, u32[]{:S(2)}) copy-start(f32[4]{0:T(128)S(1)} %get-tuple-element.23) | copy-start | bytes 52
  135.4 10.0 %copy-start.30 = (f32[4]{0:T(128)}, f32[4]{0:T(128)S(1)}, u32[]{:S(2)}) copy-start(f32[4]{0:T(128)S(1)} %broadcast_multiply_fusion) | copy-start | bytes 52
  151.3 9.5 %copy-start.13 = (bf16[256,512]{1,0:T(8,128)(2,1)S(1)}, bf16[256,512]{1,0:T(8,128)(2,1)}, u32[]{:S(2)}) copy-start(bf16[256,512]{1,0:T(8,128)(2,1)} %param.27) | copy-start | bytes 786436
  164.1 10.6 %copy-start.8 = (f32[4,256,4096]{2,1,0:T(8,128)S(1)}, f32[4,256,4096]{2,1,0:T(8,128)}, u32[]{:S(2)}) copy-start(f32[4,256,4096]{2,1,0:T(8,128)} %get-tuple-element.75) | copy-start | bytes 50331652
  174.8 8.3 %copy-start.25 = (bf16[4,1024]{1,0:T(4,128)(2,1)S(1)}, bf16[4,1024]{1,0:T(4,128)(2,1)}, u32[]{:S(2)}) copy-start(bf16[4,1024]{1,0:T(4,128)(2,1)} %param.33) | copy-start | bytes 24580
  174.8 8.4 %copy-start.17 = (f32[4,4,256]{2,1,0:T(4,128)S(1)}, f32[4,4,256]{2,1,0:T(4,128)}, u32[]{:S(2)}) copy-start(f32[4,4,256]{2,1,0:T(4,128)} %copy-done.16) | copy-start | bytes 49156
  174.8 8.6 %copy-start.15 = (f32[1024,4]{0,1:T(4,128)S(1)}, f32[1024,4]{0,1:T(4,128)}, u32[]{:S(2)}) copy-start(f32[1024,4]{0,1:T(4,128)} %copy-done.14) | copy-start | bytes 49156
  192.9 11.0 %copy-start.26 = (f32[4]{0:T(128)S(1)}, f32[4]{0:T(128)}, u32[]{:S(2)}) copy-start(f32[4]{0:T(128)} %get-tuple-element.20) | copy-start | bytes 52
  192.9 11.0 %copy-start.27 = (f32[4]{0:T(128)S(1)}, f32[4]{0:T(128)}, u32[]{:S(2)}) copy-start(f32[4]{0:T(128)} %get-tuple-element.22) | copy-start | bytes 52
  192.9 11.0 %copy-start.29 = (f32[4]{0:T(128)S(1)}, f32[4]{0:T(128)}, u32[]{:S(2)}) copy-start(f32[4]{0:T(128)} %copy-done.28) | copy-start | bytes 52
  192.9 11.0 %copy-start.31 = (f32[4]{0:T(128)S(1)}, f32[4]{0:T(128)}, u32[]{:S(2)}) copy-start(f32[4]{0:T(128)} %copy-done.30) | copy-start | bytes 52
  208.2 25.7 %copy-start.1 = (bf16[2048,768]{1,0:T(8,128)(2,1)S(1)}, bf16[2048,768]{1,0:T(8,128)(2,1)}, u32[]{:S(2)}) copy-start(bf16[2048,768]{1,0:T(8,128)(2,1)} %param.22) | copy-start | bytes 9437188
  (14 other events, 37.2 us)
Sparse Core Ops, SparseCore 0:
  25.9 96.2 all-gather.1

commit v3 on v2

--- a/solution.py
+++ b/solution.py
@@ -86,7 +86,6 @@
     counts = [{"plane": plane, "line": planes, "all": devices}[item[1]] for item in items]
     amount = len(items)
     starts = [sum(counts[:i]) for i in range(amount)]
-    whole = any(item[1] == "all" for item in items)
     shared = any(item[2] for item in items)
 
     def kernel(*refs):
@@ -102,17 +101,18 @@
             if reach == "line":
                 slot = (across + step + planes) % planes
                 return slot * plane + within, slot
-            slot = (here + step + devices) % devices
+            up, along = step // plane, step % plane
+            if step < 0:
+                up, along = -((-step) // plane), -((-step) % plane)
+            slot = (across + up + planes) % planes * plane + (within + along + plane) % plane
             return slot, slot
 
         barrier = pltpu.get_barrier_semaphore()
         greeted = 0
-        for reach in ("plane", "line", "all"):
-            if reach == "all" and not whole or reach != "all" and whole:
+        for reach in ("plane", "line"):
+            if not any(item[1] in (reach, "all") for item in items):
                 continue
-            if not any(item[1] == reach for item in items):
-                continue
-            size = {"plane": plane, "line": planes, "all": devices}[reach]
+            size = {"plane": plane, "line": planes}[reach]
             for step in range(1, size):
                 pl.semaphore_signal(
                     barrier,
@@ -138,6 +138,16 @@
         def sent(i, step):
             goal, goal_slot = place(items[i][1], step)
             mine = place(items[i][1], 0)[1]
+            if items[i][1] == "all" and step % plane and step >= plane:
+                from_line = place("all", -(step // plane * plane))[1]
+                return pltpu.make_async_remote_copy(
+                    src_ref=target(i, from_line, core),
+                    dst_ref=target(i, from_line, core),
+                    send_sem=send.at[starts[i] + step],
+                    recv_sem=recv.at[starts[i] + step],
+                    device_id=(place("plane", step % plane)[0], core),
+                    device_id_type=pl.DeviceIdType.MESH,
+                )
             return pltpu.make_async_remote_copy(
                 src_ref=ins[i].at[goal_slot] if items[i][3] else ins[i],
                 dst_ref=target(i, mine, core),
@@ -173,8 +183,11 @@
 
         kept = []
         for i in range(amount):
-            for step in range(1, counts[i]):
-                sent(i, step).start()
+            if items[i][1] == "all":
+                for up in range(1, planes):
+                    sent(i, up * plane).start()
+                for step in range(1, plane):
+                    sent(i, step).start()
         for i in range(amount):
             slot = place(items[i][1], 0)[1]
             local = pltpu.make_async_copy(
@@ -186,7 +199,21 @@
                 for turn in range(1, cores):
                     passed(i, 0, turn, True).start()
         for i in range(amount):
+            if items[i][1] == "all":
+                for up in range(1, planes):
+                    arrived(i, up * plane).wait_recv()
+                    for step in range(up * plane + 1, (up + 1) * plane):
+                        sent(i, step).start()
+                    for turn in range(1, cores):
+                        passed(i, up * plane, turn, True).start()
+        for i in range(amount):
+            if items[i][1] != "all":
+                for step in range(1, counts[i]):
+                    sent(i, step).start()
+        for i in range(amount):
             for step in range(1, counts[i]):
+                if items[i][1] == "all" and step % plane == 0:
+                    continue
                 arrived(i, step).wait_recv()
                 if items[i][2]:
                     for turn in range(1, cores):
@@ -252,48 +279,92 @@
     return (scaled * gain.reshape(groups, -1)[None]).reshape(length, -1).astype(jnp.bfloat16)
 
 
-def attend_piece(
-    carry,
-    query_plain,
-    query_turned,
-    query_positions,
-    latent,
-    key_turned,
-    key_positions,
-    key_up,
-    value_up_weight,
-):
-    highest, total, summed = carry
-    heads = query_plain.shape[1]
-    count = latent.shape[0]
-    key_plain = (
-        jnp.dot(latent, key_up, preferred_element_type=jnp.float32)
-        .astype(jnp.bfloat16)
-        .reshape(count, heads, -1)
-    )
-    values = (
-        jnp.dot(latent, value_up_weight, preferred_element_type=jnp.float32)
-        .astype(jnp.bfloat16)
-        .reshape(count, heads, -1)
-    )
-    scale = (query_plain.shape[-1] + query_turned.shape[-1]) ** (-0.5)
-    query_whole = jnp.concatenate([query_plain, query_turned], axis=-1)
-    shared_turned = jnp.broadcast_to(key_turned[:, None, :], (count, heads, key_turned.shape[-1]))
-    key_whole = jnp.concatenate([key_plain, shared_turned], axis=-1)
-    scores = (
-        jnp.einsum("qhd,khd->hqk", query_whole, key_whole, preferred_element_type=jnp.float32)
-        * scale
-    )
-    scores = jnp.where(
-        key_positions[None, None, :] <= query_positions[None, :, None], scores, -jnp.inf
-    )
-    new_highest = jnp.maximum(highest, jnp.max(scores, axis=-1))
-    weights = jnp.exp(scores - new_highest[..., None])
-    total = jnp.sum(weights, axis=-1)
-    summed = jnp.einsum(
-        "hqk,khd->hqd", weights.astype(jnp.bfloat16), values, preferred_element_type=jnp.float32
-    )
-    return (new_highest, total, summed)
+def attend(query, cosine, sine, keys, key_up, value_up_weight, length):
+    heads = key_up.shape[1] // UNROTATED_WIDTH
+    latent_width = key_up.shape[0]
+    whole = UNROTATED_WIDTH + ROPE
+    half = ROPE // 2
+    step = 2 * length if keys.shape[0] % (2 * length) == 0 else length
+    scale = whole ** (-0.5)
+    contract = (((1,), (1,)), ((), ()))
+
+    def kernel(q_ref, cos_ref, sin_ref, k_ref, ku_ref, vu_ref, out_ref, q_all, top, total, summed):
+        start = lax.axis_index("sp") * length
+        for h in range(heads):
+            base = h * whole
+            turn = q_ref[:, base + UNROTATED_WIDTH : base + whole].astype(jnp.float32)
+            first, second = turn[:, :half], turn[:, half:]
+            turned = jnp.concatenate(
+                [
+                    first * cos_ref[...] - second * sin_ref[...],
+                    second * cos_ref[...] + first * sin_ref[...],
+                ],
+                axis=1,
+            )
+            q_all[h] = jnp.concatenate(
+                [q_ref[:, base : base + UNROTATED_WIDTH], turned.astype(jnp.bfloat16)], axis=1
+            )
+        top[...] = jnp.full(top.shape, floor_score, jnp.float32)
+        total[...] = jnp.zeros(total.shape, jnp.float32)
+        summed[...] = jnp.zeros(summed.shape, jnp.float32)
+        row = start + lax.broadcasted_iota(jnp.int32, (length, step), 0)
+        column = lax.broadcasted_iota(jnp.int32, (length, step), 1)
+
+        def visit(j, carry):
+            at = pl.ds(pl.multiple_of(j * step, step), step)
+            latent = k_ref[at, :latent_width]
+            turned = k_ref[at, latent_width : latent_width + ROPE]
+            seen = column + j * step <= row
+            for h in range(heads):
+                col = slice(h * UNROTATED_WIDTH, (h + 1) * UNROTATED_WIDTH)
+                val = slice(h * VALUE_WIDTH, (h + 1) * VALUE_WIDTH)
+                plain = jnp.dot(
+                    latent, ku_ref[:, col], preferred_element_type=jnp.float32
+                ).astype(jnp.bfloat16)
+                values = jnp.dot(
+                    latent, vu_ref[:, val], preferred_element_type=jnp.float32
+                ).astype(jnp.bfloat16)
+                key = jnp.concatenate([plain, turned], axis=1)
+                scores = (
+                    lax.dot_general(q_all[h], key, contract, preferred_element_type=jnp.float32)
+                    * scale
+                )
+                scores = jnp.where(seen, scores, -jnp.inf)
+                old = top[h][:, :1]
+                new = jnp.maximum(old, jnp.max(scores, axis=1, keepdims=True))
+                weights = jnp.exp(scores - new)
+                shrink = jnp.exp(old - new)
+                now = jnp.sum(weights, axis=1, keepdims=True)
+                total[h] = total[h] * shrink + now
+                summed[h] = summed[h] * shrink + jnp.dot(
+                    weights.astype(jnp.bfloat16), values, preferred_element_type=jnp.float32
+                )
+                top[h] = jnp.broadcast_to(new, top.shape[1:])
+            return carry
+
+        lax.fori_loop(0, (start + length + step - 1) // step, visit, 0)
+        for h in range(heads):
+            out_ref[:, h * VALUE_WIDTH : (h + 1) * VALUE_WIDTH] = (
+                summed[h] / total[h][:, :1]
+            ).astype(jnp.bfloat16)
+
+    return pl.pallas_call(
+        kernel,
+        out_shape=jax.ShapeDtypeStruct((length, heads * VALUE_WIDTH), jnp.bfloat16),
+        in_specs=[pl.BlockSpec(memory_space=pltpu.VMEM)] * 6,
+        out_specs=pl.BlockSpec(memory_space=pltpu.VMEM),
+        scratch_shapes=[
+            pltpu.VMEM((heads, length, whole), jnp.bfloat16),
+            pltpu.VMEM((heads, length, 128), jnp.float32),
+            pltpu.VMEM((heads, length, 128), jnp.float32),
+            pltpu.VMEM((heads, length, VALUE_WIDTH), jnp.float32),
+        ],
+        compiler_params=pltpu.CompilerParams(vmem_limit_bytes=40 * 1024 * 1024),
+        cost_estimate=pl.CostEstimate(
+            flops=4 * 10**10, bytes_accessed=4 * 2**20, transcendentals=0
+        ),
+        name="attend",
+    )(query, cosine, sine, keys, key_up, value_up_weight)
 
 
 def shards(
@@ -382,33 +453,12 @@
     edge_rows = from_behind(all_rows[plane * length - 8 :], "sp", plane)
     positions = sp_index * length + jnp.arange(length, dtype=jnp.int32)
     rows = lax.dynamic_slice_in_dim(all_rows, within * length, length, 0)
-    heads = key_up.shape[1] // UNROTATED_WIDTH
-
     query = jnp.dot(rows, query_proj, preferred_element_type=jnp.float32).astype(jnp.bfloat16)
-    query = query.reshape(length, heads, UNROTATED_WIDTH + ROPE)
-    query_plain = query[:, :, :UNROTATED_WIDTH]
-    query_turned = rotate(query[:, :, UNROTATED_WIDTH:].astype(jnp.float32), positions).astype(
-        jnp.bfloat16
-    )
-    initial = (
-        jnp.full((heads, length), floor_score, jnp.float32),
-        jnp.zeros((heads, length), jnp.float32),
-        jnp.zeros((heads, length, VALUE_WIDTH), jnp.float32),
-    )
-    key_positions = jnp.arange(all_keys.shape[0], dtype=jnp.int32)
-    _, total, summed = attend_piece(
-        initial,
-        query_plain,
-        query_turned,
-        positions,
-        all_keys[:, :latent_width],
-        all_keys[:, latent_width : latent_width + ROPE],
-        key_positions,
-        key_up,
-        value_up_weight,
-    )
-    attended = jnp.transpose((summed / total[..., None]).astype(jnp.bfloat16), (1, 0, 2)).reshape(
-        length, heads * VALUE_WIDTH
+    half = ROPE // 2
+    freqs = theta ** (-jnp.arange(half, dtype=jnp.float32) * 2.0 / ROPE)
+    angle = positions.astype(jnp.float32)[:, None] * freqs[None, :]
+    attended = attend(
+        query, jnp.cos(angle), jnp.sin(angle), all_keys, key_up, value_up_weight, length
     )
 
     def own_part(array, axis, size):

time: 242 us -> 203 us (0.84)
  starting transfers between devices: 27.3 us -> 3.92 us
  matrix products: 41.5 us -> 18.9 us
  Pallas kernels: 94.1 us -> 110 us
  other arithmetic: 24.1 us -> 18.9 us
  local copies, waits for them, and re-layouts: 39 us -> 35.1 us
    ppermute x1, starting transfers between devices: 27.3 us -> 3.88 us  [from_behind(): lax.ppermute(value, axis, [(source, source + steps) for source in range(i...]
    dot_general x4 -> x0, matrix products: 22.8 us -> none  [the longest x1 9.48 us: attend_piece(): jnp.einsum('qhd,khd->hqk', query_whole, key_whole, preferred_element_type...]
    pallas_call x4, Pallas kernels: 94.1 us -> 105 us  [exchange(): pl.pallas_call(kernel, out_shape=shapes, in_specs=[pl.BlockSpec(memory_sp...]
    reduce_sum x1 -> x0, other arithmetic: 8.57 us -> none  [attend_piece(): total = jnp.sum(weights, axis=-1)]
    pallas_call x0 -> x1, Pallas kernels: none -> 5.15 us  [attend(): pl.pallas_call(kernel, out_shape=jax.ShapeDtypeStruct((length, heads * VA...]
    slice x3 -> x0, local copies, waits for them, and re-layouts: 5.11 us -> none  [the longest x2 3.39 us: shards(): all_keys[:, latent_width:latent_width + ROPE]]
    reshape x2, local copies, waits for them, and re-layouts: 0.97 us -> 4.95 us  [shards(): head_conv.reshape(plane, length, own_groups, per_group, SSM_DIM)]
    mul x3, other arithmetic: 0.09 us -> 2.69 us  [short_conv(): taps[index].astype(jnp.float32)[None, :] * padded[index:index + length]]
  transfers between devices with their start and end apart: 2 -> 2, of which waited for: 0 -> 0; matrix products, arithmetic and copies ran while one was open for 30% -> 16% of each run, Pallas kernels for 24% -> 27%
where the time goes in v3:
time: 203 us; the launch traced here: 202 us
  Pallas kernels  110 us (54%)
  local copies, waits for them, and re-layouts  35.1 us (17%)
  other arithmetic  18.9 us (9%)
  matrix products  18.9 us (9%)
  between operations  14.8 us (7%)
  starting transfers between devices  3.92 us (2%)
    pallas_call x4, Pallas kernels, exchange(): pl.pallas_call(kernel, out_shape=shapes, in_specs=[pl.BlockSpec(memory_sp...  105 us
    unnamed x90, local copies, waits for them, and re-layouts  10.3 us
    dot_general x1, matrix products, shards(): jnp.dot(all_rows, weights, preferred_element_type=jnp.float32)  6.71 us
    another operation x2, local copies, waits for them, and re-layouts, gated_norm(): flat = mixed.reshape(length, groups, -1)  5.95 us
    pallas_call x1, Pallas kernels, attend(): pl.pallas_call(kernel, out_shape=jax.ShapeDtypeStruct((length, heads * VA...  5.15 us
    reshape x2, local copies, waits for them, and re-layouts, shards(): head_conv.reshape(plane, length, own_groups, per_group, SSM_DIM)  4.95 us
  transfers between devices with their start and end apart: 2, of which 0 were waited for; matrix products, arithmetic and copies ran while one was open for 16% of the time, Pallas kernels for 27%

profile of v3, /device:TPU:0, one launch (start us, length us, event | category | flops | bytes accessed | tf_op | source)
XLA Modules:
  0.0 201.7 jit_solution(5450978042515437649)
XLA Ops:
  11.2 13.8 %weights_in_plane.1 = bf16[4,128,768]{2,1,0:T(8,128)(2,1)S(1)} custom-call(bf16[4,128,768]{2,1,0:T(8,128)(2,1)S(1)} %pad_maximum_fusion.refs_0_), custom_call_target="tpu_custom_call" | custom-call | flops 100000000 | bytes 4194304 | tf_op jit(solution)/shard_map/weights_in_plane/pallas_call | solution.py:237
  29.5 1.8 fusion.7
  32.1 50.1 %rows_and_keys.1 = (bf16[16,2,128,384]{3,2,1,0:T(8,128)(2,1)S(1)}, bf16[4,2,128,2048]{3,2,1,0:T(8,128)(2,1)S(1)}, f32[4,16,256]{2,1,0:T(8,128)S(1)}) custom-call(bf16[128,384]{1,0:T(8,128)(2,1)S(1)} %maximum_maximum_fusion.refs_0_, bf16[128,2048]{1,0:T(8,128)(2,1)S(1)} %fusion.17.refs_1_, f32[16,256]{1,0:T(8,128)S(1)} %bitcast.126), custom_call_target="tpu_custom_call" | custom-call | flops 100000000 | bytes 4194304 | tf_op jit(solution)/shard_map/rows_and_keys/pallas_call | solution.py:237
  82.2 1.7 copy-done.5
  83.9 2.0 copy-done.1
  86.5 3.9 %collective-permute-start = (bf16[8,2048]{1,0:T(8,128)(2,1)}, bf16[8,2048]{1,0:T(8,128)(2,1)}, u32[]{:S(2)}, u32[]{:S(2)}) collective-permute-start(bf16[8,2048]{1,0:T(8,128)(2,1)} %slice.263), channel_id=1, source_target_pairs={{0,8},{2,10},{4,12},{6,14},{8,16},{10,18},{12,20},{14,22},{16,24},... | collective-permute-start | bytes 98312 | tf_op jit(solution)/shard_map/ppermute | solution.py:23
  90.9 3.4 %compare_select_fusion = f32[1024,4]{0,1:T(4,128)S(1)} fusion(bf16[1024,2048]{1,0:T(8,128)(2,1)} %bitcast.120, bf16[2048,32]{0,1:T(8,128)(2,1)} %param.32, s32[]{:T(128)S(6)} %select_n.58), kind=kOutput, calls=%fused_computation.114 | convolution fusion | flops 16801792 | bytes 4227076 | tf_op jit(solution)/shard_map/dot_general | solution.py:470
  102.1 1.5 dynamic_slice.35
  103.6 1.5 fusion.74
  107.6 2.2 %convolution_convert_fusion.1.q_ref = bf16[256,768]{1,0:T(8,128)(2,1)S(1)} fusion(bf16[2048,768]{1,0:T(8,128)(2,1)S(1)} %copy-done, bf16[1024,2048]{1,0:T(8,128)(2,1)} %bitcast.121, s32[]{:T(128)S(6)} %select_n.55), kind=kOutput, calls=%fused_computation.24 | convolution fusion | flops 805502976 | bytes 4587524 | tf_op jit(solution)/shard_map/dot_general | solution.py:456
  109.9 5.2 %attend.1 = bf16[256,512]{1,0:T(8,128)(2,1)} custom-call(bf16[256,768]{1,0:T(8,128)(2,1)S(1)} %convolution_convert_fusion.1.q_ref, f32[256,32]{1,0:T(8,128)S(1)} %get-tuple-element.61.cos_ref, f32[256,32]{1,0:T(8,128)S(1)} %get-tuple-element.60.sin_ref, bf16[4096,384]{1,0:T(8,128)(2,1)S(1)} %bitcast.127, bf16[256,512]{1,0:T(8,128)(2,1)S(1)} %copy-done.7, ...), custom_call_target="tpu_custom_call" | custom-call | flops 40000000000 | bytes 4194304 | tf_op jit(solution)/shard_map/attend/pallas_call | solution.py:351
  115.0 6.7 %convolution_convert_fusion = bf16[1024,768]{1,0:T(8,128)(2,1)S(1)} fusion(bf16[1024,2048]{1,0:T(8,128)(2,1)} %bitcast.122, bf16[2048,768]{1,0:T(8,128)(2,1)} %all-gather.2.cloned.1.call-done), kind=kOutput, calls=%fused_computation.8 | convolution fusion | flops 3222011904 | bytes 8912896 | tf_op jit(solution)/shard_map/dot_general | solution.py:484
  124.7 1.4 multiply_convert_fusion.3
  126.1 2.8 %reshape.322 = bf16[4,256,1,4,64]{4,3,1,0,2:T(4,128)(2,1)} reshape(bf16[1024,256]{1,0:T(8,128)(2,1)} %multiply_convert_fusion.3) | data formatting | bytes 1048576 | tf_op jit(solution)/shard_map/reshape | solution.py:503
  128.9 2.2 %copy.55 = bf16[4,256,1,4,64]{1,4,3,0,2:T(8,128)(2,1)} copy(bf16[4,256,1,4,64]{4,3,1,0,2:T(4,128)(2,1)} %reshape.322) | data formatting | bytes 1048576 | tf_op jit(solution)/shard_map/reshape | solution.py:503
  133.6 26.1 %states.1 = (bf16[4,256,128]{2,1,0:T(8,128)(2,1)S(1)}, f32[4,8,128]{2,1,0:T(8,128)S(1)}) custom-call(bf16[256,128]{1,0:T(8,128)(2,1)S(1)} %fusion.48.refs_0_, f32[8,128]{1,0:T(8,128)S(1)} %pad.4.refs_1_), custom_call_target="tpu_custom_call" | custom-call | flops 100000000 | bytes 4194304 | tf_op jit(solution)/shard_map/states/pallas_call | solution.py:237
  164.2 1.3 fusion.14
  165.5 2.7 %copy.65 = f32[4,256,1,4,64]{4,3,1,0,2:T(4,128)} copy(f32[4,256,1,4,64]{1,4,3,0,2:T(8,128)} %fusion.14) | data formatting | bytes 2097152 | tf_op jit(solution)/shard_map/reshape;reshape | solution.py:276
  168.2 3.2 %reshape.323 = f32[1024,256]{1,0:T(8,128)} reshape(f32[4,256,1,4,64]{4,3,1,0,2:T(4,128)} %copy.65) | data formatting | bytes 2097152 | tf_op jit(solution)/shard_map/reshape;reshape | solution.py:276
  171.4 1.8 multiply_reduce_fusion
  173.2 1.7 multiply_convert_fusion.2
  175.0 15.0 %outputs_in_plane.1 = bf16[4,256,256]{2,1,0:T(8,128)(2,1)S(1)} custom-call(bf16[4,256,256]{2,1,0:T(8,128)(2,1)S(1)} %bitcast.125), custom_call_target="tpu_custom_call" | custom-call | flops 100000000 | bytes 4194304 | tf_op jit(solution)/shard_map/outputs_in_plane/pallas_call | solution.py:237
  190.8 2.1 %copy.58 = bf16[256,4,256]{0,2,1:T(8,128)(2,1)} copy(bf16[256,4,256]{2,0,1:T(8,128)(2,1)} %bitcast.124) | data formatting | bytes 1048576 | tf_op jit(solution)/shard_map/transpose | solution.py:565
  192.8 2.0 %copy.59 = bf16[256,1024]{1,0:T(8,128)(2,1)} copy(bf16[256,1024]{0,1:T(8,128)(2,1)} %bitcast.132) | data formatting | bytes 1048576
  (159 shorter events, 30.9 us)
Async XLA Ops:
  7.2 100.5 %copy-start = (bf16[2048,768]{1,0:T(8,128)(2,1)S(1)}, bf16[2048,768]{1,0:T(8,128)(2,1)}, u32[]{:S(2)}) copy-start(bf16[2048,768]{1,0:T(8,128)(2,1)} %param.22) | copy-start | bytes 9437188
  7.2 107.9 %all-gather.2.cloned.1.call-start = ((), (), s32[]{:S(2)}) async-start(), calls=%async_computation | async-start | bytes 3932160 | tf_op jit(solution)/shard_map/all_gather | solution.py:420
  11.0 16.3 %copy-start.17 = (bf16[2048,64]{0,1:T(8,128)(2,1)S(1)}, bf16[2048,64]{0,1:T(8,128)(2,1)}, u32[]{:S(2)}) copy-start(bf16[2048,64]{0,1:T(8,128)(2,1)} %param.25) | copy-start | bytes 786436
  11.0 17.2 %copy-start.20 = (f32[2048]{0:T(1024)S(1)}, f32[2048]{0:T(1024)}, u32[]{:S(2)}) copy-start(f32[2048]{0:T(1024)} %param.21) | copy-start | bytes 24580
  25.9 5.8 %copy-start.38 = (f32[256]{0:T(256)S(1)}, f32[256]{0:T(256)}, u32[]{:S(2)}) copy-start(f32[256]{0:T(256)} %param.24) | copy-start | bytes 3076
  26.0 6.1 %copy-start.31 = (f32[32]{0:T(128)}, f32[32]{0:T(128)S(1)}, u32[]{:S(2)}) copy-start(f32[32]{0:T(128)S(1)} %multiply_power_fusion) | copy-start | bytes 388
  26.0 6.1 %copy-start.4 = (f32[256,16]{0,1:T(8,128)S(1)}, f32[256,16]{0,1:T(8,128)}, u32[]{:S(2)}) copy-start(f32[256,16]{0,1:T(8,128)} %param.37) | copy-start | bytes 49156
  32.0 62.4 %copy-start.43 = (f32[16]{0:T(128)S(1)}, f32[16]{0:T(128)}, u32[]{:S(2)}) copy-start(f32[16]{0:T(128)} %param.36) | copy-start | bytes 196
  86.5 36.1 %collective-permute-start = (bf16[8,2048]{1,0:T(8,128)(2,1)}, bf16[8,2048]{1,0:T(8,128)(2,1)}, u32[]{:S(2)}, u32[]{:S(2)}) collective-permute-start(bf16[8,2048]{1,0:T(8,128)(2,1)} %slice.263), channel_id=1, source_target_pairs={{0,8},{2,10},{4,12},{6,14},{8,16},{10,18},{12,20},{14,22},{16,24},... | collective-permute-start | bytes 98312 | tf_op jit(solution)/shard_map/ppermute | solution.py:23
  94.5 15.4 %copy-start.7 = (bf16[256,512]{1,0:T(8,128)(2,1)S(1)}, bf16[256,512]{1,0:T(8,128)(2,1)}, u32[]{:S(2)}) copy-start(bf16[256,512]{1,0:T(8,128)(2,1)} %ku_ref.1) | copy-start | bytes 786436
  96.2 3.1 %copy-start.34 = (f32[4]{0:T(128)}, f32[4]{0:T(128)S(1)}, u32[]{:S(2)}) copy-start(f32[4]{0:T(128)S(1)} %get-tuple-element.21) | copy-start | bytes 52
  102.1 13.0 %copy-start.39 = (pred[4]{0:T(512)(128)(4,1)}, pred[4]{0:T(512)(128)(4,1)S(1)}, u32[]{:S(2)}) copy-start(pred[4]{0:T(512)(128)(4,1)S(1)} %iota_compare_fusion.3) | copy-start | bytes 16
  102.1 7.8 %copy-start.6 = (bf16[16,2,128,384]{3,2,1,0:T(8,128)(2,1)S(1)}, bf16[16,2,128,384]{3,2,1,0:T(8,128)(2,1)}, u32[]{:S(2)}) copy-start(bf16[16,2,128,384]{3,2,1,0:T(8,128)(2,1)} %copy-done.5) | copy-start | bytes 9437188
  102.1 7.8 %copy-start.8 = (bf16[256,512]{1,0:T(8,128)(2,1)S(1)}, bf16[256,512]{1,0:T(8,128)(2,1)}, u32[]{:S(2)}) copy-start(bf16[256,512]{1,0:T(8,128)(2,1)} %vu_ref.1) | copy-start | bytes 786436
  115.0 7.6 %copy-start.13 = (bf16[2048,768]{1,0:T(8,128)(2,1)S(1)}, bf16[2048,768]{1,0:T(8,128)(2,1)}, u32[]{:S(2)}) copy-start(bf16[2048,768]{1,0:T(8,128)(2,1)} %all-gather.2.cloned.1.call-done) | copy-start | bytes 9437188
  121.7 2.9 %copy-start.14 = (bf16[1024,768]{1,0:T(8,128)(2,1)}, bf16[1024,768]{1,0:T(8,128)(2,1)S(1)}, u32[]{:S(2)}) copy-start(bf16[1024,768]{1,0:T(8,128)(2,1)S(1)} %convolution_convert_fusion) | copy-start | bytes 4718596
  124.7 6.4 %copy-start.26 = (bf16[3,128]{1,0:T(4,128)(2,1)S(1)}, bf16[3,128]{1,0:T(4,128)(2,1)}, u32[]{:S(2)}) copy-start(bf16[3,128]{1,0:T(4,128)(2,1)} %get-tuple-element.54) | copy-start | bytes 2308
  131.1 28.6 %copy-start.41 = (pred[4,4]{1,0:T(4,128)(4,1)S(1)}, pred[4,4]{1,0:T(4,128)(4,1)}, u32[]{:S(2)}) copy-start(pred[4,4]{1,0:T(4,128)(4,1)} %fusion.70) | copy-start | bytes 52
  131.1 28.7 %copy-start.40 = (pred[4]{0:T(512)(128)(4,1)S(1)}, pred[4]{0:T(512)(128)(4,1)}, u32[]{:S(2)}) copy-start(pred[4]{0:T(512)(128)(4,1)} %copy-done.39) | copy-start | bytes 16
  131.2 29.1 %copy-start.25 = (bf16[3,128]{1,0:T(4,128)(2,1)S(1)}, bf16[3,128]{1,0:T(4,128)(2,1)}, u32[]{:S(2)}) copy-start(bf16[3,128]{1,0:T(4,128)(2,1)} %get-tuple-element.55) | copy-start | bytes 2308
  132.3 27.5 %copy-start.15 = (bf16[1024,128]{1,0:T(8,128)(2,1)}, bf16[1024,128]{1,0:T(8,128)(2,1)S(1)}, u32[]{:S(2)}) copy-start(bf16[1024,128]{1,0:T(8,128)(2,1)S(1)} %multiply_convert_fusion.4) | copy-start | bytes 786436
  133.4 29.3 %copy-start.19 = (f32[4,4,256]{2,1,0:T(4,128)S(1)}, f32[4,4,256]{2,1,0:T(4,128)}, u32[]{:S(2)}) copy-start(f32[4,4,256]{2,1,0:T(4,128)} %copy-done.18) | copy-start | bytes 49156
  160.1 2.6 %copy-start.10 = (bf16[4,256,1,4,64]{1,4,3,0,2:T(8,128)(2,1)S(1)}, bf16[4,256,1,4,64]{1,4,3,0,2:T(8,128)(2,1)}, u32[]{:S(2)}) copy-start(bf16[4,256,1,4,64]{1,4,3,0,2:T(8,128)(2,1)} %copy.55) | copy-start | bytes 1572868
  168.2 5.0 %copy-start.24 = (f32[256]{0:T(256)S(1)}, f32[256]{0:T(256)}, u32[]{:S(2)}) copy-start(f32[256]{0:T(256)} %dynamic_slice.35) | copy-start | bytes 3076
  (22 other events, 34.1 us)
Sparse Core Ops, SparseCore 0:
  26.1 70.3 all-gather.1

commit v4 on v3

--- a/solution.py
+++ b/solution.py
@@ -80,7 +80,7 @@
     return running, state, within
 
 
-def exchange(items, plane, name, number):
+def exchange(items, plane, name, number, columns=False):
     devices, cores = lax.axis_size("sp"), lax.axis_size("tp")
     planes = devices // plane
     counts = [{"plane": plane, "line": planes, "all": devices}[item[1]] for item in items]
@@ -133,6 +133,9 @@
         pl.semaphore_wait(barrier, greeted)
 
         def target(i, slot, who):
+            if columns:
+                size = ins[i].shape[-1]
+                return outs[i].at[:, pl.ds(pl.multiple_of(slot * size, size), size)]
             return outs[i].at[slot, who] if items[i][2] else outs[i].at[slot]
 
         def sent(i, step):
@@ -189,6 +192,10 @@
                 for step in range(1, plane):
                     sent(i, step).start()
         for i in range(amount):
+            if items[i][1] != "all":
+                for step in range(1, counts[i]):
+                    sent(i, step).start()
+        for i in range(amount):
             slot = place(items[i][1], 0)[1]
             local = pltpu.make_async_copy(
                 ins[i].at[slot] if items[i][3] else ins[i], target(i, slot, core), own.at[i]
@@ -206,10 +213,6 @@
                         sent(i, step).start()
                     for turn in range(1, cores):
                         passed(i, up * plane, turn, True).start()
-        for i in range(amount):
-            if items[i][1] != "all":
-                for step in range(1, counts[i]):
-                    sent(i, step).start()
         for i in range(amount):
             for step in range(1, counts[i]):
                 if items[i][1] == "all" and step % plane == 0:
@@ -232,6 +235,8 @@
     for (array, reach, over, selected), count in zip(items, counts):
         lead = (count, cores) if over else (count,)
         tail = array.shape[1:] if selected else array.shape
+        if columns:
+            lead, tail = (), (tail[0], count * tail[1])
         shapes.append(jax.ShapeDtypeStruct(lead + tail, array.dtype))
     slots = sum(counts)
     return pl.pallas_call(
@@ -315,16 +320,17 @@
             latent = k_ref[at, :latent_width]
             turned = k_ref[at, latent_width : latent_width + ROPE]
             seen = column + j * step <= row
+            plain = jnp.dot(latent, ku_ref[...], preferred_element_type=jnp.float32).astype(
+                jnp.bfloat16
+            )
+            all_values = jnp.dot(latent, vu_ref[...], preferred_element_type=jnp.float32).astype(
+                jnp.bfloat16
+            )
             for h in range(heads):
-                col = slice(h * UNROTATED_WIDTH, (h + 1) * UNROTATED_WIDTH)
-                val = slice(h * VALUE_WIDTH, (h + 1) * VALUE_WIDTH)
-                plain = jnp.dot(
-                    latent, ku_ref[:, col], preferred_element_type=jnp.float32
-                ).astype(jnp.bfloat16)
-                values = jnp.dot(
-                    latent, vu_ref[:, val], preferred_element_type=jnp.float32
-                ).astype(jnp.bfloat16)
-                key = jnp.concatenate([plain, turned], axis=1)
+                values = all_values[:, h * VALUE_WIDTH : (h + 1) * VALUE_WIDTH]
+                key = jnp.concatenate(
+                    [plain[:, h * UNROTATED_WIDTH : (h + 1) * UNROTATED_WIDTH], turned], axis=1
+                )
                 scores = (
                     lax.dot_general(q_all[h], key, contract, preferred_element_type=jnp.float32)
                     * scale
@@ -398,8 +404,10 @@
     own_groups = groups // plane
     direct = plane > 1
 
-    def move(items, name, number):
-        return exchange(items, plane, name, number) if direct else plain_exchange(items, plane)
+    def move(items, name, number, columns=False):
+        if direct:
+            return exchange(items, plane, name, number, columns)
+        return plain_exchange(items, plane)
 
     depth = scan_input.shape[0]
     widths = [w.shape[1] // plane for w in (scan_input, scan_gate, scan_write, scan_read)]
@@ -560,9 +568,9 @@
     ).reshape(plane * length, own_groups, per_group, SSM_DIM)
     scanned = gated_norm(mixed, gate, own_part(group_gain, 0, widths[0]))
     (columns,) = move(
-        [(scanned.reshape(plane, length, -1), "plane", False, True)], "outputs_in_plane", 4
-    )
-    scanned = jnp.transpose(columns, (1, 0, 2)).reshape(length, -1)
+        [(scanned.reshape(plane, length, -1), "plane", False, True)], "outputs_in_plane", 4, True
+    )
+    scanned = columns.reshape(length, -1)
     return (attended, scanned)
 
 

time: 203 us -> 187 us (0.921)
  Pallas kernels: 110 us -> 99.3 us
  local copies, waits for them, and re-layouts: 35.1 us -> 31.1 us
    pallas_call x4, Pallas kernels: 105 us -> 94.8 us  [exchange(): pl.pallas_call(kernel, out_shape=shapes, in_specs=[pl.BlockSpec(memory_sp...]
    unnamed x90 -> x88, local copies, waits for them, and re-layouts: 10.3 us -> 8.21 us
    transpose x1 -> x0, local copies, waits for them, and re-layouts: 2.05 us -> none  [shards(): scanned = jnp.transpose(columns, (1, 0, 2)).reshape(length, -1)]
  transfers between devices with their start and end apart: 2 -> 2, of which waited for: 0 -> 0; matrix products, arithmetic and copies ran while one was open for 16% -> 18% of each run, Pallas kernels for 27% -> 29%
where the time goes in v4:
time: 187 us; the launch traced here: 186 us
  Pallas kernels  99.3 us (53%)
  local copies, waits for them, and re-layouts  31.1 us (17%)
  other arithmetic  19 us (10%)
  matrix products  18.9 us (10%)
  between operations  14.8 us (8%)
  starting transfers between devices  3.11 us (2%)
    pallas_call x4, Pallas kernels, exchange(): pl.pallas_call(kernel, out_shape=shapes, in_specs=[pl.BlockSpec(memory_sp...  94.8 us
    unnamed x88, local copies, waits for them, and re-layouts  8.21 us
    dot_general x1, matrix products, shards(): jnp.dot(all_rows, weights, preferred_element_type=jnp.float32)  6.7 us
    another operation x2, local copies, waits for them, and re-layouts, gated_norm(): flat = mixed.reshape(length, groups, -1)  5.96 us
    reshape x2, local copies, waits for them, and re-layouts, shards(): head_conv.reshape(plane, length, own_groups, per_group, SSM_DIM)  4.96 us
    pallas_call x1, Pallas kernels, attend(): pl.pallas_call(kernel, out_shape=jax.ShapeDtypeStruct((length, heads * VA...  4.45 us
  transfers between devices with their start and end apart: 2, of which 0 were waited for; matrix products, arithmetic and copies ran while one was open for 18% of the time, Pallas kernels for 29%

profile of v4, /device:TPU:0, one launch (start us, length us, event | category | flops | bytes accessed | tf_op | source)
XLA Modules:
  0.0 186.1 jit_solution(546445621517097332)
XLA Ops:
  11.2 13.6 %weights_in_plane.1 = bf16[4,128,768]{2,1,0:T(8,128)(2,1)S(1)} custom-call(bf16[4,128,768]{2,1,0:T(8,128)(2,1)S(1)} %pad_maximum_fusion.refs_0_), custom_call_target="tpu_custom_call" | custom-call | flops 100000000 | bytes 4194304 | tf_op jit(solution)/shard_map/weights_in_plane/pallas_call | solution.py:242
  29.3 1.8 fusion.7
  31.9 50.2 %rows_and_keys.1 = (bf16[16,2,128,384]{3,2,1,0:T(8,128)(2,1)S(1)}, bf16[4,2,128,2048]{3,2,1,0:T(8,128)(2,1)S(1)}, f32[4,16,256]{2,1,0:T(8,128)S(1)}) custom-call(bf16[128,384]{1,0:T(8,128)(2,1)S(1)} %maximum_maximum_fusion.refs_0_, bf16[128,2048]{1,0:T(8,128)(2,1)S(1)} %fusion.17.refs_1_, f32[16,256]{1,0:T(8,128)S(1)} %bitcast.123), custom_call_target="tpu_custom_call" | custom-call | flops 100000000 | bytes 4194304 | tf_op jit(solution)/shard_map/rows_and_keys/pallas_call | solution.py:242
  82.1 1.7 copy-done.4
  83.8 1.9 %copy-done.1 = bf16[4,2,128,2048]{3,2,1,0:T(8,128)(2,1)} copy-done((bf16[4,2,128,2048]{3,2,1,0:T(8,128)(2,1)}, bf16[4,2,128,2048]{3,2,1,0:T(8,128)(2,1)S(1)}, u32[]{:S(2)}) %copy-start.1) | copy-done | bytes 4194328
  86.4 3.1 %collective-permute-start = (bf16[8,2048]{1,0:T(8,128)(2,1)}, bf16[8,2048]{1,0:T(8,128)(2,1)}, u32[]{:S(2)}, u32[]{:S(2)}) collective-permute-start(bf16[8,2048]{1,0:T(8,128)(2,1)} %slice.263), channel_id=1, source_target_pairs={{0,8},{2,10},{4,12},{6,14},{8,16},{10,18},{12,20},{14,22},{16,24},... | collective-permute-start | bytes 98312 | tf_op jit(solution)/shard_map/ppermute | solution.py:23
  90.0 3.4 %compare_select_fusion = f32[1024,4]{0,1:T(4,128)S(1)} fusion(bf16[1024,2048]{1,0:T(8,128)(2,1)} %bitcast.118, bf16[2048,32]{0,1:T(8,128)(2,1)} %param.32, s32[]{:T(128)S(6)} %select_n.58), kind=kOutput, calls=%fused_computation.114 | convolution fusion | flops 16801792 | bytes 4227076 | tf_op jit(solution)/shard_map/dot_general | solution.py:478
  97.2 1.3 dynamic_slice.34
  101.3 1.5 dynamic_slice.35
  102.8 1.4 fusion.74
  106.9 2.2 %convolution_convert_fusion.1.q_ref = bf16[256,768]{1,0:T(8,128)(2,1)S(1)} fusion(bf16[2048,768]{1,0:T(8,128)(2,1)S(1)} %copy-done, bf16[1024,2048]{1,0:T(8,128)(2,1)} %bitcast.119, s32[]{:T(128)S(6)} %select_n.55), kind=kOutput, calls=%fused_computation.24 | convolution fusion | flops 805502976 | bytes 4587524 | tf_op jit(solution)/shard_map/dot_general | solution.py:464
  109.1 4.4 %attend.1 = bf16[256,512]{1,0:T(8,128)(2,1)} custom-call(bf16[256,768]{1,0:T(8,128)(2,1)S(1)} %convolution_convert_fusion.1.q_ref, f32[256,32]{1,0:T(8,128)S(1)} %get-tuple-element.55.cos_ref, f32[256,32]{1,0:T(8,128)S(1)} %get-tuple-element.54.sin_ref, bf16[4096,384]{1,0:T(8,128)(2,1)S(1)} %bitcast.124, bf16[256,512]{1,0:T(8,128)(2,1)S(1)} %copy-done.6, ...), custom_call_target="tpu_custom_call" | custom-call | flops 40000000000 | bytes 4194304 | tf_op jit(solution)/shard_map/attend/pallas_call | solution.py:357
  113.6 6.7 %convolution_convert_fusion = bf16[1024,768]{1,0:T(8,128)(2,1)S(1)} fusion(bf16[1024,2048]{1,0:T(8,128)(2,1)} %bitcast.120, bf16[2048,768]{1,0:T(8,128)(2,1)} %all-gather.2.cloned.1.call-done), kind=kOutput, calls=%fused_computation.8 | convolution fusion | flops 3222011904 | bytes 8912896 | tf_op jit(solution)/shard_map/dot_general | solution.py:492
  121.1 1.3 convolution_convert_fusion.2
  123.2 1.4 multiply_convert_fusion.3
  124.6 2.8 %reshape.318 = bf16[4,256,1,4,64]{4,3,1,0,2:T(4,128)(2,1)} reshape(bf16[1024,256]{1,0:T(8,128)(2,1)} %multiply_convert_fusion.3) | data formatting | bytes 1048576 | tf_op jit(solution)/shard_map/reshape | solution.py:511
  127.4 2.2 %copy.51 = bf16[4,256,1,4,64]{1,4,3,0,2:T(8,128)(2,1)} copy(bf16[4,256,1,4,64]{4,3,1,0,2:T(4,128)(2,1)} %reshape.318) | data formatting | bytes 1048576 | tf_op jit(solution)/shard_map/reshape | solution.py:511
  132.1 20.3 %states.1 = (bf16[4,256,128]{2,1,0:T(8,128)(2,1)S(1)}, f32[4,8,128]{2,1,0:T(8,128)S(1)}) custom-call(bf16[256,128]{1,0:T(8,128)(2,1)S(1)} %fusion.48.refs_0_, f32[8,128]{1,0:T(8,128)S(1)} %pad.4.refs_1_), custom_call_target="tpu_custom_call" | custom-call | flops 100000000 | bytes 4194304 | tf_op jit(solution)/shard_map/states/pallas_call | solution.py:242
  156.9 1.3 fusion.14
  158.3 2.7 %copy.59 = f32[4,256,1,4,64]{4,3,1,0,2:T(4,128)} copy(f32[4,256,1,4,64]{1,4,3,0,2:T(8,128)} %fusion.14) | data formatting | bytes 2097152 | tf_op jit(solution)/shard_map/reshape;reshape | solution.py:281
  161.0 3.2 %reshape.319 = f32[1024,256]{1,0:T(8,128)} reshape(f32[4,256,1,4,64]{4,3,1,0,2:T(4,128)} %copy.59) | data formatting | bytes 2097152 | tf_op jit(solution)/shard_map/reshape;reshape | solution.py:281
  164.2 1.8 multiply_reduce_fusion
  166.0 1.7 multiply_convert_fusion.2
  167.7 10.7 %outputs_in_plane.1 = bf16[256,1024]{1,0:T(8,128)(2,1)S(1)} custom-call(bf16[4,256,256]{2,1,0:T(8,128)(2,1)S(1)} %bitcast.122), custom_call_target="tpu_custom_call" | custom-call | flops 100000000 | bytes 4194304 | tf_op jit(solution)/shard_map/outputs_in_plane/pallas_call | solution.py:242
  (156 shorter events, 28.5 us)
Async XLA Ops:
  7.2 99.7 %copy-start = (bf16[2048,768]{1,0:T(8,128)(2,1)S(1)}, bf16[2048,768]{1,0:T(8,128)(2,1)}, u32[]{:S(2)}) copy-start(bf16[2048,768]{1,0:T(8,128)(2,1)} %param.22) | copy-start | bytes 9437188
  7.2 106.4 %all-gather.2.cloned.1.call-start = ((), (), s32[]{:S(2)}) async-start(), calls=%async_computation | async-start | bytes 3932160 | tf_op jit(solution)/shard_map/all_gather | solution.py:428
  11.0 16.1 %copy-start.16 = (bf16[2048,64]{0,1:T(8,128)(2,1)S(1)}, bf16[2048,64]{0,1:T(8,128)(2,1)}, u32[]{:S(2)}) copy-start(bf16[2048,64]{0,1:T(8,128)(2,1)} %param.25) | copy-start | bytes 786436
  11.0 17.0 %copy-start.19 = (f32[2048]{0:T(1024)S(1)}, f32[2048]{0:T(1024)}, u32[]{:S(2)}) copy-start(f32[2048]{0:T(1024)} %param.21) | copy-start | bytes 24580
  25.7 5.8 %copy-start.37 = (f32[256]{0:T(256)S(1)}, f32[256]{0:T(256)}, u32[]{:S(2)}) copy-start(f32[256]{0:T(256)} %param.24) | copy-start | bytes 3076
  25.8 6.1 %copy-start.30 = (f32[32]{0:T(128)}, f32[32]{0:T(128)S(1)}, u32[]{:S(2)}) copy-start(f32[32]{0:T(128)S(1)} %multiply_power_fusion) | copy-start | bytes 388
  25.8 6.1 %copy-start.3 = (f32[256,16]{0,1:T(8,128)S(1)}, f32[256,16]{0,1:T(8,128)}, u32[]{:S(2)}) copy-start(f32[256,16]{0,1:T(8,128)} %param.37) | copy-start | bytes 49156
  31.7 61.7 %copy-start.42 = (f32[16]{0:T(128)S(1)}, f32[16]{0:T(128)}, u32[]{:S(2)}) copy-start(f32[16]{0:T(128)} %param.36) | copy-start | bytes 196
  86.4 34.8 %collective-permute-start = (bf16[8,2048]{1,0:T(8,128)(2,1)}, bf16[8,2048]{1,0:T(8,128)(2,1)}, u32[]{:S(2)}, u32[]{:S(2)}) collective-permute-start(bf16[8,2048]{1,0:T(8,128)(2,1)} %slice.263), channel_id=1, source_target_pairs={{0,8},{2,10},{4,12},{6,14},{8,16},{10,18},{12,20},{14,22},{16,24},... | collective-permute-start | bytes 98312 | tf_op jit(solution)/shard_map/ppermute | solution.py:23
  93.5 15.5 %copy-start.6 = (bf16[256,512]{1,0:T(8,128)(2,1)S(1)}, bf16[256,512]{1,0:T(8,128)(2,1)}, u32[]{:S(2)}) copy-start(bf16[256,512]{1,0:T(8,128)(2,1)} %ku_ref.1) | copy-start | bytes 786436
  95.3 3.2 %copy-start.33 = (f32[4]{0:T(128)}, f32[4]{0:T(128)S(1)}, u32[]{:S(2)}) copy-start(f32[4]{0:T(128)S(1)} %get-tuple-element.15) | copy-start | bytes 52
  101.3 12.3 %copy-start.38 = (pred[4]{0:T(512)(128)(4,1)}, pred[4]{0:T(512)(128)(4,1)S(1)}, u32[]{:S(2)}) copy-start(pred[4]{0:T(512)(128)(4,1)S(1)} %iota_compare_fusion.3) | copy-start | bytes 16
  101.3 7.8 %copy-start.5 = (bf16[16,2,128,384]{3,2,1,0:T(8,128)(2,1)S(1)}, bf16[16,2,128,384]{3,2,1,0:T(8,128)(2,1)}, u32[]{:S(2)}) copy-start(bf16[16,2,128,384]{3,2,1,0:T(8,128)(2,1)} %copy-done.4) | copy-start | bytes 9437188
  101.3 7.8 %copy-start.7 = (bf16[256,512]{1,0:T(8,128)(2,1)S(1)}, bf16[256,512]{1,0:T(8,128)(2,1)}, u32[]{:S(2)}) copy-start(bf16[256,512]{1,0:T(8,128)(2,1)} %vu_ref.1) | copy-start | bytes 786436
  113.6 7.6 %copy-start.12 = (bf16[2048,768]{1,0:T(8,128)(2,1)S(1)}, bf16[2048,768]{1,0:T(8,128)(2,1)}, u32[]{:S(2)}) copy-start(bf16[2048,768]{1,0:T(8,128)(2,1)} %all-gather.2.cloned.1.call-done) | copy-start | bytes 9437188
  120.3 2.9 %copy-start.13 = (bf16[1024,768]{1,0:T(8,128)(2,1)}, bf16[1024,768]{1,0:T(8,128)(2,1)S(1)}, u32[]{:S(2)}) copy-start(bf16[1024,768]{1,0:T(8,128)(2,1)S(1)} %convolution_convert_fusion) | copy-start | bytes 4718596
  123.2 6.4 %copy-start.25 = (bf16[3,128]{1,0:T(4,128)(2,1)S(1)}, bf16[3,128]{1,0:T(4,128)(2,1)}, u32[]{:S(2)}) copy-start(bf16[3,128]{1,0:T(4,128)(2,1)} %get-tuple-element.48) | copy-start | bytes 2308
  129.6 22.9 %copy-start.40 = (pred[4,4]{1,0:T(4,128)(4,1)S(1)}, pred[4,4]{1,0:T(4,128)(4,1)}, u32[]{:S(2)}) copy-start(pred[4,4]{1,0:T(4,128)(4,1)} %fusion.70) | copy-start | bytes 52
  129.6 23.0 %copy-start.39 = (pred[4]{0:T(512)(128)(4,1)S(1)}, pred[4]{0:T(512)(128)(4,1)}, u32[]{:S(2)}) copy-start(pred[4]{0:T(512)(128)(4,1)} %copy-done.38) | copy-start | bytes 16
  129.7 23.4 %copy-start.24 = (bf16[3,128]{1,0:T(4,128)(2,1)S(1)}, bf16[3,128]{1,0:T(4,128)(2,1)}, u32[]{:S(2)}) copy-start(bf16[3,128]{1,0:T(4,128)(2,1)} %get-tuple-element.49) | copy-start | bytes 2308
  130.8 21.7 %copy-start.14 = (bf16[1024,128]{1,0:T(8,128)(2,1)}, bf16[1024,128]{1,0:T(8,128)(2,1)S(1)}, u32[]{:S(2)}) copy-start(bf16[1024,128]{1,0:T(8,128)(2,1)S(1)} %multiply_convert_fusion.4) | copy-start | bytes 786436
  131.9 23.5 %copy-start.18 = (f32[4,4,256]{2,1,0:T(4,128)S(1)}, f32[4,4,256]{2,1,0:T(4,128)}, u32[]{:S(2)}) copy-start(f32[4,4,256]{2,1,0:T(4,128)} %copy-done.17) | copy-start | bytes 49156
  152.8 2.6 %copy-start.9 = (bf16[4,256,1,4,64]{1,4,3,0,2:T(8,128)(2,1)S(1)}, bf16[4,256,1,4,64]{1,4,3,0,2:T(8,128)(2,1)}, u32[]{:S(2)}) copy-start(bf16[4,256,1,4,64]{1,4,3,0,2:T(8,128)(2,1)} %copy.51) | copy-start | bytes 1572868
  161.0 5.0 %copy-start.23 = (f32[256]{0:T(256)S(1)}, f32[256]{0:T(256)}, u32[]{:S(2)}) copy-start(f32[256]{0:T(256)} %dynamic_slice.35) | copy-start | bytes 3076
  (21 other events, 33.2 us)
Sparse Core Ops, SparseCore 0:
  25.8 70.3 all-gather.1
